TPU v7x, 128 devices: a whole 4x4x4 slice. The times are simulated.
128 devices in a mesh: kv: 16 (over z, y), tp: 8 (over x, core).
Axes of the slice: x: 4, y: 4, z: 4, core: 2. Of those that a mesh axis runs over, the one named last changes fastest.
Arguments:
- tokens: bfloat16 [128, 4096], P(None, 'kv'), may hold values from -8 to 8
- attn_gain: float32 [4096], P('kv'), may hold values from 0.1 to 1.9
- w_query: bfloat16 [4096, 2048], P('kv', 'tp'), may hold values from -0.09375 to 0.09375
- w_key: bfloat16 [4096, 2048], P('kv', 'tp'), may hold values from -0.09375 to 0.09375
- w_value: bfloat16 [4096, 4096], P('kv', 'tp'), may hold values from -0.09375 to 0.09375
- w_outgate: bfloat16 [4096, 4096], P('kv', 'tp'), may hold values from -0.09375 to 0.09375
- w_gates: bfloat16 [4096, 16], replicated, may hold values from -0.029907227 to 0.029907227
- forget_bias: float32 [8], replicated, may hold values from -1 to 3
- state_c: float32 [128, 8, 512, 256], P('kv', 'tp'), may hold values from -6 to 6
- state_n: float32 [128, 8, 256], P('kv', 'tp'), may hold values from -6 to 6
- state_m: float32 [128, 8], P('kv', 'tp'), may hold values from -2 to 0.5
- w_output: bfloat16 [4096, 4096], P('tp', 'kv'), may hold values from -0.09375 to 0.09375
- mlp_gain: float32 [4096], P('kv'), may hold values from 0.1 to 1.9
- w_gateff: bfloat16 [4096, 11008], P('kv', 'tp'), may hold values from -0.09375 to 0.09375
- w_upff: bfloat16 [4096, 11008], P('kv', 'tp'), may hold values from -0.09375 to 0.09375
- w_downff: bfloat16 [11008, 4096], P('tp', 'kv'), may hold values from -0.0546875 to 0.0546875
Outputs:
- mixed: bfloat16 [128, 4096], P(None, 'kv')
- new_c: float32 [128, 8, 512, 256], P('kv', 'tp')
- new_n: float32 [128, 8, 256], P('kv', 'tp')
- new_m: float32 [128, 8], P('kv', 'tp')
All inputs are finite; a program needn't handle non-finite values.
Results may differ from a plain program's by a relative error of at most 0.0083.
Values may be sent and summed in bfloat16 or wider, within the bound.
A program may use at most 64 MiB of HBM per device.

v0:
```python
import jax
import jax.numpy as jnp
from jax import lax
from jax.sharding import PartitionSpec as P

norm_floor = 1e-05


def in_blocks(value, dim, length):
    dims = value.shape
    pieces = value.reshape(*dims[:dim], length, dims[dim] // length, *dims[dim + 1 :])
    return jnp.moveaxis(pieces, dim, 0)


def sum_at_owner(value, axis, dim):
    pieces = in_blocks(value, dim, lax.axis_size(axis))
    arrived = lax.all_to_all(pieces, axis, split_axis=0, concat_axis=0, tiled=True)
    return arrived.astype(jnp.float32).sum(axis=0)


def shortened(value):

    def short(part):
        return part.astype(jnp.bfloat16) if part.dtype == jnp.float32 else part

    return jax.tree.map(short, value)


def sent_to_all(value, axis):
    copies = jnp.broadcast_to(value, (lax.axis_size(axis), *value.shape))
    return lax.all_to_all(copies, axis, split_axis=0, concat_axis=0, tiled=True)


def joined_along(pieces, dim):
    pieces = jnp.moveaxis(pieces, 0, dim)
    dims = pieces.shape
    return pieces.reshape(*dims[:dim], dims[dim] * dims[dim + 1], *dims[dim + 2 :])


def collect(value, axis, dim):
    pieces = sent_to_all(value, axis)
    return joined_along(pieces, dim)


def taken_together(value, axis):
    everything = sent_to_all(value, axis)
    return jnp.sum(everything.astype(jnp.float32), axis=0)


def over_copies(value, axis):
    return sent_to_all(value, axis).sum(axis=0)


def per_device(
    tokens,
    attn_gain,
    w_query,
    w_key,
    w_value,
    w_outgate,
    w_gates,
    forget_bias,
    state_c,
    state_n,
    state_m,
    w_output,
    mlp_gain,
    w_gateff,
    w_upff,
    w_downff,
):
    kv_count = lax.axis_size("kv")
    kv_at = lax.axis_index("kv")
    tp_at = lax.axis_index("tp")
    batch = tokens.shape[0]
    width_dev = tokens.shape[1]
    width_all = width_dev * kv_count
    rows = batch // kv_count
    heads_dev = state_c.shape[1]
    heads_all = forget_bias.shape[0]
    value_size = state_c.shape[2]
    query_size = state_c.shape[3]
    tok_float = tokens.astype(jnp.float32)
    squares_one = jnp.sum(tok_float * tok_float, axis=1)
    normed_one = (tok_float * attn_gain).astype(jnp.bfloat16)
    query_width = heads_dev * query_size
    value_width = heads_dev * value_size
    stacked = jnp.concatenate([w_query, w_key, w_value, w_outgate], axis=1)
    proj_part = jnp.dot(normed_one, stacked, preferred_element_type=jnp.float32)
    gate_rows = lax.dynamic_slice_in_dim(w_gates, kv_at * width_dev, width_dev, 0)
    gate_part = jnp.dot(normed_one, gate_rows, preferred_element_type=jnp.float32)
    extra_one = (squares_one,)
    summed_one = jax.tree.map(
        lambda part: sum_at_owner(part, "kv", 0), shortened((proj_part, gate_part) + extra_one)
    )
    rows_one = summed_one[2]
    scale_one = lax.rsqrt(rows_one / width_all + norm_floor)[:, None]
    proj_rows = summed_one[0] * scale_one
    gate_all = summed_one[1] * scale_one
    query = (proj_rows[:, :query_width] * query_size ** (-0.5)).reshape(rows, heads_dev, query_size)
    key_vec = proj_rows[:, query_width : 2 * query_width].reshape(rows, heads_dev, query_size)
    value = proj_rows[:, 2 * query_width : 2 * query_width + value_width].reshape(
        rows, heads_dev, value_size
    )
    out_pre = proj_rows[:, 2 * query_width + value_width :].reshape(rows, heads_dev, value_size)
    log_input = lax.dynamic_slice_in_dim(gate_all, tp_at * heads_dev, heads_dev, 1)
    forget_pre = lax.dynamic_slice_in_dim(gate_all, heads_all + tp_at * heads_dev, heads_dev, 1)
    bias_dev = lax.dynamic_slice_in_dim(forget_bias, tp_at * heads_dev, heads_dev, 0)
    log_forget = jax.nn.log_sigmoid(forget_pre + bias_dev)
    carried = log_forget + state_m
    new_m = jnp.maximum(carried, log_input)
    keep = jnp.exp(carried - new_m)
    admit = jnp.exp(log_input - new_m)
    new_c = (
        keep[:, :, None, None] * state_c
        + admit[:, :, None, None] * value[:, :, :, None] * key_vec[:, :, None, :]
    )
    new_n = keep[:, :, None] * state_n + admit[:, :, None] * key_vec
    numer = jnp.einsum("bhvd,bhd->bhv", new_c, query, precision=lax.Precision.HIGHEST)
    denom = jnp.maximum(jnp.abs(jnp.sum(new_n * query, axis=-1)), jnp.exp(-new_m))
    head_out = (
        (jax.nn.sigmoid(out_pre) * numer / denom[:, :, None])
        .reshape(rows, value_width)
        .astype(jnp.bfloat16)
    )
    attn_part = jnp.dot(collect(head_out, "kv", 0), w_output, preferred_element_type=jnp.float32)
    attn_mix = taken_together(attn_part.astype(jnp.bfloat16), "tp").astype(jnp.float32)
    middle = (tok_float + attn_mix).astype(jnp.bfloat16)
    mid_float = middle.astype(jnp.float32)
    squares_two = jnp.sum(mid_float * mid_float, axis=1)
    normed_two = (mid_float * mlp_gain).astype(jnp.bfloat16)
    gate_ff = jnp.dot(normed_two, w_gateff, preferred_element_type=jnp.float32)
    up_ff = jnp.dot(normed_two, w_upff, preferred_element_type=jnp.float32)
    extra_two = (squares_two,)
    summed_two = jax.tree.map(
        lambda part: sum_at_owner(part, "kv", 0), shortened((gate_ff, up_ff) + extra_two)
    )
    rows_two = summed_two[2]
    scale_two = lax.rsqrt(rows_two / width_all + norm_floor)[:, None]
    hidden_ff = (jax.nn.silu(summed_two[0] * scale_two) * (summed_two[1] * scale_two)).astype(
        jnp.bfloat16
    )
    down_part = jnp.dot(collect(hidden_ff, "kv", 0), w_downff, preferred_element_type=jnp.float32)
    down_sum = over_copies(down_part, "tp")
    mixed = (mid_float + down_sum).astype(jnp.bfloat16)
    return (mixed, new_c, new_n, new_m)


def solution(mesh):
    placed = (
        P(None, "kv"),
        P("kv"),
        P("kv", "tp"),
        P("kv", "tp"),
        P("kv", "tp"),
        P("kv", "tp"),
        P(),
        P(),
        P("kv", "tp", None, None),
        P("kv", "tp", None),
        P("kv", "tp"),
        P("tp", "kv"),
        P("kv"),
        P("kv", "tp"),
        P("kv", "tp"),
        P("tp", "kv"),
    )
    return jax.shard_map(
        per_device,
        mesh=mesh,
        in_specs=placed,
        out_specs=(P(None, "kv"), P("kv", "tp", None, None), P("kv", "tp", None), P("kv", "tp")),
        check_vma=False,
    )
```

profile of v0, /device:TPU:1, one launch (start us, length us, event | category | flops | bytes accessed | tf_op | source)
XLA Modules:
  0.0 150.8 jit_solution(17463970850615773686)
XLA Ops:
  0.7 1.0 fusion.13
  2.4 8.6 %all-to-all-start.1 = ((bf16[16,1,8]{2,1,0:T(2,128)(2,1)}), bf16[16,1,8]{2,1,0:T(2,128)(2,1)S(1)}, u32[]{:S(2)}, u32[]{:S(2)}) async-start(bf16[16,1,8]{2,1,0:T(2,128)(2,1)} %convert_element_type.114), calls=%async_computation.1 | async-start | bytes 16384 | tf_op jit(solution)/shard_map/all_to_all | solution.py:17
  11.7 1.0 convolution_convert_fusion.4
  12.7 2.2 %fusion.2 = bf16[16,8,1536]{2,1,0:T(8,128)(2,1)} fusion(bf16[256,512]{1,0:T(8,128)(2,1)} %param.21, bf16[256,512]{1,0:T(8,128)(2,1)} %param.20, bf16[256,256]{1,0:T(8,128)(2,1)} %param.19, bf16[256,256]{1,0:T(8,128)(2,1)} %param.18, bf16[128,256]{1,0:T(8,128)(2,1)} %param.16, f32[256]{0:T(256)} %param.17), kind=kOutput, calls=%fused_computation.6 | convolution fusion | flops 104103936 | bytes 1246208 | tf_op jit(solution)/shard_map/dot_general | solution.py:89
  15.6 1.2 dynamic_slice.14
  17.3 6.2 %all-to-all-start.2 = ((bf16[16,8,16]{2,1,0:T(8,128)(2,1)}), bf16[16,8,16]{2,1,0:T(8,128)(2,1)S(1)}, u32[]{:S(2)}, u32[]{:S(2)}) async-start(bf16[16,8,16]{2,1,0:T(8,128)(2,1)} %bitcast.1), calls=%async_computation.2 | async-start | bytes 65536 | tf_op jit(solution)/shard_map/all_to_all | solution.py:17
  23.6 6.4 %all-to-all-done.2 = bf16[16,8,16]{2,1,0:T(8,128)(2,1)S(1)} async-done(((bf16[16,8,16]{2,1,0:T(8,128)(2,1)}), bf16[16,8,16]{2,1,0:T(8,128)(2,1)S(1)}, u32[]{:S(2)}, u32[]{:S(2)}) %all-to-all-start.2) | async-done | bytes 4128 | tf_op jit(solution)/shard_map/all_to_all | solution.py:17
  30.0 3.6 %all-to-all-start = ((bf16[16,8,1536]{2,1,0:T(8,128)(2,1)}), bf16[16,8,1536]{2,1,0:T(8,128)(2,1)S(1)}, u32[]{:S(2)}, u32[]{:S(2)}) async-start(bf16[16,8,1536]{2,1,0:T(8,128)(2,1)} %fusion.2), calls=%async_computation | async-start | bytes 786432 | tf_op jit(solution)/shard_map/all_to_all | solution.py:17
  34.5 7.2 %all-to-all-done = bf16[16,8,1536]{2,1,0:T(8,128)(2,1)S(1)} async-done(((bf16[16,8,1536]{2,1,0:T(8,128)(2,1)}), bf16[16,8,1536]{2,1,0:T(8,128)(2,1)S(1)}, u32[]{:S(2)}, u32[]{:S(2)}) %all-to-all-start) | async-done | bytes 393248 | tf_op jit(solution)/shard_map/all_to_all | solution.py:17
  42.9 2.6 %multiply_add_fusion = f32[8,1,512,256]{3,2,1,0:T(8,128)S(1)} fusion(f32[8,1,512,256]{3,2,1,0:T(8,128)} %param.24, f32[8,256]{1,0:T(8,128)S(1)} %get-tuple-element.26, f32[8,512]{1,0:T(8,128)S(1)} %slice_multiply_fusion, f32[8]{0:T(128)S(1)} %get-tuple-element.16), kind=kLoop, calls=%fused_computation.2 | loop fusion | flops 3145728 | bytes 8413216 | tf_op jit(solution)/shard_map/add | solution.py:115
  45.6 2.0 %copy-done.1 = f32[8,1,512,256]{3,2,1,0:T(8,128)} copy-done((f32[8,1,512,256]{3,2,1,0:T(8,128)}, f32[8,1,512,256]{3,2,1,0:T(8,128)S(1)}, u32[]{:S(2)}) %copy-start.1) | copy-done | bytes 4194328
  47.6 3.6 %fusion = f32[8,1,512]{2,1,0:T(1,128)S(1)} fusion(f32[8,1,512,256]{3,2,1,0:T(8,128)S(1)} %multiply_add_fusion, f32[8,256,1]{1,0,2:T(8,128)S(1)} %get-tuple-element.24), kind=kOutput, calls=%fused_computation | convolution fusion | flops 12582912 | bytes 4218880 | tf_op jit(solution)/shard_map/bhvd,bhd->bhv/dot_general | solution.py:119
  51.3 9.6 %all_to_all.52 = bf16[16,8,512]{2,1,0:T(8,128)(2,1)S(1)} all-to-all(bf16[16,8,512]{2,1,0:T(8,128)(2,1)S(1)} %broadcast_in_dim.8), channel_id=1, replica_groups=mesh['kv'=16,'tp'=8] {'kv'}, dimensions={0} | all-to-all | bytes 262144 | tf_op jit(solution)/shard_map/all_to_all | solution.py:31
  61.1 18.5 %all_to_all.53 = bf16[8,128,256]{2,1,0:T(8,128)(2,1)S(1)} all-to-all(bf16[8,128,256]{2,1,0:T(8,128)(2,1)S(1)} %broadcast_in_dim.9), channel_id=1, replica_groups=mesh['kv'=16,'tp'=8] {'tp'}, dimensions={0} | all-to-all | bytes 1048576 | tf_op jit(solution)/shard_map/all_to_all | solution.py:31
  80.6 3.5 %all-to-all-start.6 = ((bf16[16,1,8]{2,1,0:T(2,128)(2,1)}), bf16[16,1,8]{2,1,0:T(2,128)(2,1)S(1)}, u32[]{:S(2)}, u32[]{:S(2)}) async-start(bf16[16,1,8]{2,1,0:T(2,128)(2,1)} %convert_element_type.115), calls=%async_computation.6 | async-start | bytes 16384 | tf_op jit(solution)/shard_map/all_to_all | solution.py:17
  85.3 5.0 %all-to-all-done.6 = bf16[16,1,8]{2,1,0:T(2,128)(2,1)S(1)} async-done(((bf16[16,1,8]{2,1,0:T(2,128)(2,1)}), bf16[16,1,8]{2,1,0:T(2,128)(2,1)S(1)}, u32[]{:S(2)}, u32[]{:S(2)}) %all-to-all-start.6) | async-done | bytes 288 | tf_op jit(solution)/shard_map/all_to_all | solution.py:17
  90.3 3.5 %all-to-all-start.7 = ((bf16[16,8,1376]{2,1,0:T(8,128)(2,1)}), bf16[16,8,1376]{2,1,0:T(8,128)(2,1)S(1)}, u32[]{:S(2)}, u32[]{:S(2)}) async-start(bf16[16,8,1376]{2,1,0:T(8,128)(2,1)} %bitcast.10), calls=%async_computation.7 | async-start | bytes 720896 | tf_op jit(solution)/shard_map/all_to_all | solution.py:17
  95.2 6.8 %all-to-all-done.7 = bf16[16,8,1376]{2,1,0:T(8,128)(2,1)S(1)} async-done(((bf16[16,8,1376]{2,1,0:T(8,128)(2,1)}), bf16[16,8,1376]{2,1,0:T(8,128)(2,1)S(1)}, u32[]{:S(2)}, u32[]{:S(2)}) %all-to-all-start.7) | async-done | bytes 352288 | tf_op jit(solution)/shard_map/all_to_all | solution.py:17
  102.0 3.5 %all-to-all-start.5 = ((bf16[16,8,1376]{2,1,0:T(8,128)(2,1)}), bf16[16,8,1376]{2,1,0:T(8,128)(2,1)S(1)}, u32[]{:S(2)}, u32[]{:S(2)}) async-start(bf16[16,8,1376]{2,1,0:T(8,128)(2,1)} %bitcast.9), calls=%async_computation.5 | async-start | bytes 720896 | tf_op jit(solution)/shard_map/all_to_all | solution.py:17
  105.6 8.1 %all-to-all-done.5 = bf16[16,8,1376]{2,1,0:T(8,128)(2,1)S(1)} async-done(((bf16[16,8,1376]{2,1,0:T(8,128)(2,1)}), bf16[16,8,1376]{2,1,0:T(8,128)(2,1)S(1)}, u32[]{:S(2)}, u32[]{:S(2)}) %all-to-all-start.5) | async-done | bytes 352288 | tf_op jit(solution)/shard_map/all_to_all | solution.py:17
  113.9 10.7 %all_to_all.54 = bf16[16,8,1376]{2,1,0:T(8,128)(2,1)S(1)} all-to-all(bf16[16,8,1376]{2,1,0:T(8,128)(2,1)S(1)} %broadcast_in_dim.10), channel_id=1, replica_groups=mesh['kv'=16,'tp'=8] {'kv'}, dimensions={0} | all-to-all | bytes 704512 | tf_op jit(solution)/shard_map/all_to_all | solution.py:31
  124.8 1.1 broadcast_in_dim.11
  125.9 9.2 %all-to-all-start.9 = ((f32[8,128,256]{2,1,0:T(8,128)}), f32[8,128,256]{2,1,0:T(8,128)S(1)}, u32[]{:S(2)}, u32[]{:S(2)}) async-start(f32[8,128,256]{2,1,0:T(8,128)} %broadcast_in_dim.11), calls=%async_computation.9 | async-start | bytes 2097152 | tf_op jit(solution)/shard_map/all_to_all | solution.py:31
  135.7 14.4 %all-to-all-done.9 = f32[8,128,256]{2,1,0:T(8,128)S(1)} async-done(((f32[8,128,256]{2,1,0:T(8,128)}), f32[8,128,256]{2,1,0:T(8,128)S(1)}, u32[]{:S(2)}, u32[]{:S(2)}) %all-to-all-start.9) | async-done | bytes 1048608 | tf_op jit(solution)/shard_map/all_to_all | solution.py:31
  (53 shorter events, 10.4 us)
Async XLA Ops:
  0.6 83.4 %copy-start = (bf16[256,1376]{0,1:T(8,128)(2,1)S(1)}, bf16[256,1376]{0,1:T(8,128)(2,1)}, u32[]{:S(2)}) copy-start(bf16[256,1376]{0,1:T(8,128)(2,1)} %param.30) | copy-start | bytes 2113540
  0.6 41.4 %copy-start.6 = (f32[8,1,256]{2,1,0:T(1,128)S(1)}, f32[8,1,256]{2,1,0:T(1,128)}, u32[]{:S(2)}) copy-start(f32[8,1,256]{2,1,0:T(1,128)} %param.25) | copy-start | bytes 24580
  2.4 15.0 %all-to-all-start.1 = ((bf16[16,1,8]{2,1,0:T(2,128)(2,1)}), bf16[16,1,8]{2,1,0:T(2,128)(2,1)S(1)}, u32[]{:S(2)}, u32[]{:S(2)}) async-start(bf16[16,1,8]{2,1,0:T(2,128)(2,1)} %convert_element_type.114), calls=%async_computation.1 | async-start | bytes 16384 | tf_op jit(solution)/shard_map/all_to_all | solution.py:17
  17.3 12.6 %all-to-all-start.2 = ((bf16[16,8,16]{2,1,0:T(8,128)(2,1)}), bf16[16,8,16]{2,1,0:T(8,128)(2,1)S(1)}, u32[]{:S(2)}, u32[]{:S(2)}) async-start(bf16[16,8,16]{2,1,0:T(8,128)(2,1)} %bitcast.1), calls=%async_computation.2 | async-start | bytes 65536 | tf_op jit(solution)/shard_map/all_to_all | solution.py:17
  30.0 11.8 %all-to-all-start = ((bf16[16,8,1536]{2,1,0:T(8,128)(2,1)}), bf16[16,8,1536]{2,1,0:T(8,128)(2,1)S(1)}, u32[]{:S(2)}, u32[]{:S(2)}) async-start(bf16[16,8,1536]{2,1,0:T(8,128)(2,1)} %fusion.2), calls=%async_computation | async-start | bytes 786432 | tf_op jit(solution)/shard_map/all_to_all | solution.py:17
  45.5 2.0 %copy-start.1 = (f32[8,1,512,256]{3,2,1,0:T(8,128)}, f32[8,1,512,256]{3,2,1,0:T(8,128)S(1)}, u32[]{:S(2)}) copy-start(f32[8,1,512,256]{3,2,1,0:T(8,128)S(1)} %multiply_add_fusion) | copy-start | bytes 12582916
  45.6 15.3 %copy-start.4 = (bf16[512,256]{1,0:T(8,128)(2,1)S(1)}, bf16[512,256]{1,0:T(8,128)(2,1)}, u32[]{:S(2)}) copy-start(bf16[512,256]{1,0:T(8,128)(2,1)} %param.27) | copy-start | bytes 786436
  45.6 34.2 %copy-start.5 = (bf16[128,256]{1,0:T(8,128)(2,1)S(1)}, bf16[128,256]{1,0:T(8,128)(2,1)}, u32[]{:S(2)}) copy-start(bf16[128,256]{1,0:T(8,128)(2,1)} %param.16) | copy-start | bytes 196612
  45.6 38.5 %copy-start.7 = (f32[256]{0:T(256)S(1)}, f32[256]{0:T(256)}, u32[]{:S(2)}) copy-start(f32[256]{0:T(256)} %param.28) | copy-start | bytes 3076
  47.6 46.3 %copy-start.2 = (bf16[256,1376]{0,1:T(8,128)(2,1)S(1)}, bf16[256,1376]{0,1:T(8,128)(2,1)}, u32[]{:S(2)}) copy-start(bf16[256,1376]{0,1:T(8,128)(2,1)} %param.29) | copy-start | bytes 2113540
  79.7 44.9 %copy-start.3 = (bf16[1376,256]{1,0:T(8,128)(2,1)S(1)}, bf16[1376,256]{1,0:T(8,128)(2,1)}, u32[]{:S(2)}) copy-start(bf16[1376,256]{1,0:T(8,128)(2,1)} %param.31) | copy-start | bytes 2113540
  80.6 9.8 %all-to-all-start.6 = ((bf16[16,1,8]{2,1,0:T(2,128)(2,1)}), bf16[16,1,8]{2,1,0:T(2,128)(2,1)S(1)}, u32[]{:S(2)}, u32[]{:S(2)}) async-start(bf16[16,1,8]{2,1,0:T(2,128)(2,1)} %convert_element_type.115), calls=%async_computation.6 | async-start | bytes 16384 | tf_op jit(solution)/shard_map/all_to_all | solution.py:17
  90.3 11.7 %all-to-all-start.7 = ((bf16[16,8,1376]{2,1,0:T(8,128)(2,1)}), bf16[16,8,1376]{2,1,0:T(8,128)(2,1)S(1)}, u32[]{:S(2)}, u32[]{:S(2)}) async-start(bf16[16,8,1376]{2,1,0:T(8,128)(2,1)} %bitcast.10), calls=%async_computation.7 | async-start | bytes 720896 | tf_op jit(solution)/shard_map/all_to_all | solution.py:17
  102.0 11.7 %all-to-all-start.5 = ((bf16[16,8,1376]{2,1,0:T(8,128)(2,1)}), bf16[16,8,1376]{2,1,0:T(8,128)(2,1)S(1)}, u32[]{:S(2)}, u32[]{:S(2)}) async-start(bf16[16,8,1376]{2,1,0:T(8,128)(2,1)} %bitcast.9), calls=%async_computation.5 | async-start | bytes 720896 | tf_op jit(solution)/shard_map/all_to_all | solution.py:17
  125.9 24.2 %all-to-all-start.9 = ((f32[8,128,256]{2,1,0:T(8,128)}), f32[8,128,256]{2,1,0:T(8,128)S(1)}, u32[]{:S(2)}, u32[]{:S(2)}) async-start(f32[8,128,256]{2,1,0:T(8,128)} %broadcast_in_dim.11), calls=%async_computation.9 | async-start | bytes 2097152 | tf_op jit(solution)/shard_map/all_to_all | solution.py:31
where the time goes:
time: 152 us; the launch traced here: 151 us
  waiting for transfers between devices  48.4 us (32%)
  blocking collectives  38.8 us (26%)
  starting transfers between devices  38.1 us (25%)
  local copies, waits for them, and re-layouts  9.79 us (6%)
  matrix products  7.97 us (5%)
  other arithmetic  6.94 us (5%)
    all_to_all x3, blocking collectives, sent_to_all(): return lax.all_to_all(copies, axis, split_axis=0, concat_axis=0, tiled=True)  38.8 us
    all_to_all x6, waiting for transfers between devices, sum_at_owner(): lax.all_to_all(pieces, axis, split_axis=0, concat_axis=0, tiled=True)  34 us
    all_to_all x6, starting transfers between devices, sum_at_owner(): lax.all_to_all(pieces, axis, split_axis=0, concat_axis=0, tiled=True)  28.9 us
    all_to_all x1, waiting for transfers between devices, sent_to_all(): return lax.all_to_all(copies, axis, split_axis=0, concat_axis=0, tiled=True)  14.4 us
    all_to_all x1, starting transfers between devices, sent_to_all(): return lax.all_to_all(copies, axis, split_axis=0, concat_axis=0, tiled=True)  9.19 us
    convert_element_type x5, local copies, waits for them, and re-layouts, short(): return part.astype(jnp.bfloat16) if part.dtype == jnp.float32 else part  3.98 us
    dot_general x1, matrix products, per_device(): jnp.einsum('bhvd,bhd->bhv', new_c, query, precision=lax.Precision.HIGHEST)  3.63 us
    unnamed x18, local copies, waits for them, and re-layouts  3.33 us
  transfers between devices with their start and end apart: 7, of which 7 were waited for; matrix products, arithmetic and copies ran while one was open for 7% of the time, Pallas kernels for 0%

commit v1 on v0

v1 whole, which is shorter than its diff:
```python
import functools

import jax
import jax.numpy as jnp
from jax import lax
from jax.experimental import pallas as pl
from jax.experimental.pallas import tpu as pltpu
from jax.sharding import PartitionSpec as P

MESH = pl.DeviceIdType.MESH
norm_floor = 1e-05
f32 = jnp.float32
bf16 = jnp.bfloat16
LANES = 128


def up_to_lanes(length):
    return (length + LANES - 1) // LANES * LANES


def dot(a, b):
    return jnp.dot(a, b, preferred_element_type=f32)


def dot_rows(a, b):
    return lax.dot_general(a, b, (((1,), (1,)), ((), ())), preferred_element_type=f32)


def lane_ids(rows):
    return lax.broadcasted_iota(jnp.int32, (rows, LANES), 1)


def layer(
    kv_n,
    tp_n,
    tokens,
    attn_gain,
    w_query,
    w_key,
    w_value,
    w_outgate,
    w_gates,
    forget_bias,
    state_c,
    state_n,
    state_m,
    w_output,
    mlp_gain,
    w_gateff,
    w_upff,
    w_downff,
    mixed,
    new_c,
    new_n,
    new_m,
    tok_v,
    gain_one_v,
    w_proj_v,
    w_gates_v,
    bias_v,
    c_v,
    n_v,
    m_v,
    w_out_v,
    gain_two_v,
    w_gateff_v,
    w_upff_v,
    w_down_v,
    c_short,
    c_new,
    n_new,
    m_new,
    proj_send,
    proj_recv,
    head_all,
    attn_send,
    attn_recv,
    mid_all,
    ff_send,
    ff_recv,
    hidden_all,
    down_send,
    down_recv,
    mixed_all,
    in_sem,
    out_sem,
    kv_send_sem,
    kv_recv_sem,
    tp_send_sem,
    tp_recv_sem,
):
    kv = lax.axis_index("kv")
    tp = lax.axis_index("tp")
    batch, width = tok_v.shape
    rows = batch // kv_n
    tp_rows = batch // tp_n
    width_all = width * kv_n
    heads_all = bias_v.shape[1]
    value_size, query_size = c_v.shape[1:]
    proj_width = w_proj_v.shape[1]
    ff = w_gateff_v.shape[0]
    ff_pad = up_to_lanes(ff)

    loads = []

    def load(source, target):
        copy = pltpu.make_async_copy(source, target, in_sem.at[len(loads)])
        copy.start()
        loads.append(copy)
        return copy

    first = [load(tokens, tok_v), load(attn_gain, gain_one_v)]
    at = 0
    for weight in (w_query, w_key, w_value, w_outgate):
        columns = weight.shape[1]
        first.append(load(weight, w_proj_v.at[:, pl.ds(at, columns)]))
        at += columns
    first.append(load(w_gates.at[:, pl.ds(pl.multiple_of(kv * width, width), width)], w_gates_v))
    load_c = load(state_c.at[:, 0], c_v)
    load_cell = [load(state_n, n_v), load(state_m, m_v), load(forget_bias, bias_v)]
    load_out = load(w_output, w_out_v)
    load_ff = [load(mlp_gain, gain_two_v), load(w_gateff, w_gateff_v), load(w_upff, w_upff_v)]
    load_down = load(w_downff, w_down_v)

    barrier = pltpu.get_barrier_semaphore()

    def greet_kv(step, carry):
        pl.semaphore_signal(
            barrier, inc=1, device_id={"kv": lax.rem(kv + step, kv_n)}, device_id_type=MESH
        )
        return carry

    def greet_tp(step, carry):
        pl.semaphore_signal(
            barrier, inc=1, device_id={"tp": lax.rem(tp + step, tp_n)}, device_id_type=MESH
        )
        return carry

    lax.fori_loop(1, kv_n, greet_kv, 0)
    lax.fori_loop(1, tp_n, greet_tp, 0)

    def exchange(axis, phase, source_of, target):
        me, count = (kv, kv_n) if axis == "kv" else (tp, tp_n)
        sends, recvs = (kv_send_sem, kv_recv_sem) if axis == "kv" else (tp_send_sem, tp_recv_sem)

        def copy_to(peer):
            return pltpu.make_async_remote_copy(
                src_ref=source_of(peer),
                dst_ref=target.at[me],
                send_sem=sends.at[phase, peer],
                recv_sem=recvs.at[phase, me],
                device_id={axis: peer},
                device_id_type=MESH,
            )

        def copy_from(peer):
            return pltpu.make_async_remote_copy(
                src_ref=source_of(peer),
                dst_ref=target.at[peer],
                send_sem=sends.at[phase, peer],
                recv_sem=recvs.at[phase, peer],
                device_id={axis: peer},
                device_id_type=MESH,
            )

        def start(step, carry):
            copy_to(lax.rem(me + step, count)).start()
            return carry

        lax.fori_loop(1, count, start, 0)

        def arrived(step):
            peer = lax.rem(me + step, count)
            copy_from(peer).wait_recv()
            return peer

        def all_arrived():
            def wait(step, carry):
                arrived(step)
                return carry

            lax.fori_loop(1, count, wait, 0)

        def sent():
            def wait(step, carry):
                copy_to(lax.rem(me + step, count)).wait_send()
                return carry

            lax.fori_loop(1, count, wait, 0)

        def total(own):
            def add(step, carry):
                return carry + target[arrived(step)].astype(f32)

            return lax.fori_loop(1, count, add, own)

        return all_arrived, total, sent

    for copy in first:
        copy.wait()
    tok_float = tok_v[...].astype(f32)
    squares_one = jnp.sum(tok_float * tok_float, axis=1, keepdims=True)
    normed_one = (tok_float * gain_one_v[...]).astype(bf16)
    lanes = lane_ids(batch)
    gate_row = lax.broadcasted_iota(jnp.int32, (LANES, 2 * heads_all), 1)
    gate_lane = lax.broadcasted_iota(jnp.int32, (LANES, 2 * heads_all), 0)
    wanted = jnp.where(
        (gate_lane == 0) | (gate_lane == 3),
        tp,
        jnp.where((gate_lane == 1) | (gate_lane == 4), heads_all + tp, -1),
    )
    pick = jnp.where(gate_row == wanted, 1.0, 0.0).astype(bf16)
    gate_weight = dot(pick, w_gates_v[...]).astype(bf16)
    extra = dot_rows(normed_one, gate_weight)
    extra = jnp.where((lanes == 2) | (lanes == 5), squares_one, extra)
    extra_short = extra.astype(bf16).astype(f32)
    extra = jnp.where(lanes < 3, extra_short, extra - extra_short)
    proj_send[:, :, pl.ds(proj_width, LANES)] = extra.reshape(kv_n, rows, LANES).astype(bf16)
    step = 512
    for at in range(0, proj_width, step):
        part = dot(normed_one, w_proj_v[:, pl.ds(at, step)])
        proj_send[:, :, pl.ds(at, step)] = part.reshape(kv_n, rows, step).astype(bf16)

    pl.semaphore_wait(barrier, kv_n + tp_n - 2)
    _, proj_total, proj_sent = exchange("kv", 0, lambda peer: proj_send.at[peer], proj_recv)

    load_c.wait()
    for one in range(rows):
        c_short[one] = c_v[one].astype(bf16)
    for copy in load_cell:
        copy.wait()

    proj_rows = proj_total(proj_send[kv].astype(f32))
    extra = proj_rows[:, proj_width:]
    lanes = lane_ids(rows)

    def picked(lane):
        chosen = (lanes == lane) | (lanes == lane + 3)
        return jnp.sum(jnp.where(chosen, extra, 0.0), axis=1, keepdims=True)

    scale_one = lax.rsqrt(picked(2) / width_all + norm_floor)
    proj_rows = proj_rows[:, :proj_width] * scale_one
    query = proj_rows[:, :query_size] * query_size ** (-0.5)
    key_vec = proj_rows[:, query_size : 2 * query_size]
    value = proj_rows[:, 2 * query_size : 2 * query_size + value_size]
    out_pre = proj_rows[:, 2 * query_size + value_size :]
    head_lane = lax.broadcasted_iota(jnp.int32, (1, heads_all), 1)
    bias = jnp.sum(jnp.where(head_lane == tp, bias_v[...], 0.0), axis=1, keepdims=True)
    log_input = picked(0) * scale_one
    forget_pre = picked(1) * scale_one + bias
    log_forget = -(jnp.maximum(-forget_pre, 0.0) + jnp.log1p(jnp.exp(-jnp.abs(forget_pre))))
    row_at = lax.broadcasted_iota(jnp.int32, (rows, rows), 0)
    same = row_at == lax.broadcasted_iota(jnp.int32, (rows, rows), 1)
    m_column = jnp.sum(jnp.where(same, m_v[...], 0.0), axis=1, keepdims=True)
    carried = log_forget + m_column
    m_next = jnp.maximum(carried, log_input)
    keep = jnp.exp(carried - m_next)
    admit = jnp.exp(log_input - m_next)
    n_next = keep * n_v[:, 0, :] + admit * key_vec
    denom = jnp.maximum(
        jnp.abs(jnp.sum(n_next * query, axis=1, keepdims=True)), jnp.exp(-m_next)
    )
    key_query = jnp.sum(key_vec * query, axis=1, keepdims=True)
    query_short = query.astype(bf16)
    query_rest = (query - query_short.astype(f32)).astype(bf16)
    row_ids = lax.broadcasted_iota(jnp.int32, (rows, value_size), 0)
    read = jnp.zeros((rows, value_size), f32)
    query_both = jnp.concatenate([query_short.astype(f32), query_rest.astype(f32)], axis=0).astype(bf16)
    for one in range(rows):
        product = dot_rows(query_both, c_short[one])
        read = jnp.where(row_ids == one, product[:rows] + product[rows:], read)
    admitted = admit * value
    numer = keep * read + admitted * key_query
    head_all[kv] = (jax.nn.sigmoid(out_pre) * numer / denom).astype(bf16)
    head_arrived, _, head_sent = exchange("kv", 1, lambda peer: head_all.at[kv], head_all)

    n_new[:, 0, :] = n_next
    m_new[...] = jnp.sum(jnp.where(same, m_next, 0.0), axis=0, keepdims=True)
    stores = [
        pltpu.make_async_copy(n_new, new_n, out_sem.at[0]),
        pltpu.make_async_copy(m_new, new_m, out_sem.at[1]),
    ]
    for copy in stores:
        copy.start()
    admitted_column = admitted.T
    for one in range(rows):
        c_new[one] = (
            keep[one : one + 1, :] * c_v[one]
            + admitted_column[:, one : one + 1] * key_vec[one : one + 1, :]
        )
        copy = pltpu.make_async_copy(c_new.at[one], new_c.at[one, 0], out_sem.at[2 + one])
        copy.start()
        stores.append(copy)

    load_out.wait()
    head_arrived()
    heads = head_all[...].astype(f32).reshape(batch, value_size).astype(bf16)
    attn_part = dot(heads, w_out_v[...])
    attn_send[...] = attn_part.reshape(tp_n, tp_rows, width).astype(bf16)
    _, attn_total, attn_sent = exchange("tp", 0, lambda peer: attn_send.at[peer], attn_recv)
    own_rows = pl.ds(pl.multiple_of(tp * tp_rows, tp_rows), tp_rows)
    attn_mix = attn_total(attn_send[tp].astype(f32))
    mid_all[tp] = (tok_v[own_rows, :].astype(f32) + attn_mix).astype(bf16)
    mid_arrived, _, mid_sent = exchange("tp", 1, lambda peer: mid_all.at[tp], mid_all)
    for copy in load_ff:
        copy.wait()
    mid_arrived()

    mid_float = mid_all[...].astype(f32).reshape(batch, width)
    squares_two = jnp.sum(mid_float * mid_float, axis=1, keepdims=True)
    normed_two = (mid_float * gain_two_v[...]).astype(bf16)
    lanes = lane_ids(batch)
    squares_short = squares_two.astype(bf16).astype(f32)
    extra = jnp.where(
        lanes == 0, squares_short, jnp.where(lanes == 1, squares_two - squares_short, 0.0)
    )
    ff_send[:, :, pl.ds(2 * ff_pad, LANES)] = extra.reshape(kv_n, rows, LANES).astype(bf16)
    for base, weight in ((0, w_gateff_v), (ff_pad, w_upff_v)):
        for at in range(0, ff, step):
            columns = min(step, ff - at)
            part = dot_rows(normed_two, weight[pl.ds(at, columns), :])
            ff_send[:, :, pl.ds(base + at, columns)] = part.reshape(kv_n, rows, columns).astype(bf16)
    _, ff_total, ff_sent = exchange("kv", 2, lambda peer: ff_send.at[peer], ff_recv)
    ff_rows = ff_total(ff_send[kv].astype(f32))
    rows_two = jnp.sum(ff_rows[:, 2 * ff_pad :], axis=1, keepdims=True)
    scale_two = lax.rsqrt(rows_two / width_all + norm_floor)
    gate_ff = ff_rows[:, :ff] * scale_two
    up_ff = ff_rows[:, ff_pad : ff_pad + ff] * scale_two
    hidden_all[kv] = (gate_ff / (1.0 + jnp.exp(-gate_ff)) * up_ff).astype(bf16)
    hidden_arrived, _, hidden_sent = exchange("kv", 3, lambda peer: hidden_all.at[kv], hidden_all)

    load_down.wait()
    hidden_arrived()
    hidden = hidden_all[...].astype(f32).reshape(batch, ff).astype(bf16)
    down_part = dot(hidden, w_down_v[...])
    down_send[...] = down_part.reshape(tp_n, tp_rows, width).astype(bf16)
    _, down_total, down_sent = exchange("tp", 2, lambda peer: down_send.at[peer], down_recv)
    down_sum = down_total(down_send[tp].astype(f32))
    mixed_all[tp] = (mid_all[tp].astype(f32) + down_sum).astype(bf16)
    mixed_arrived, _, mixed_sent = exchange("tp", 3, lambda peer: mixed_all.at[tp], mixed_all)
    for sent in (proj_sent, head_sent, attn_sent, mid_sent, ff_sent, hidden_sent, down_sent):
        sent()
    for copy in stores:
        copy.wait()
    mixed_arrived()
    for slot in range(tp_n):
        pltpu.make_async_copy(
            mixed_all.at[slot], mixed.at[pl.ds(slot * tp_rows, tp_rows)], in_sem.at[slot]
        ).start()
    for slot in range(tp_n):
        pltpu.make_async_copy(
            mixed_all.at[slot], mixed.at[pl.ds(slot * tp_rows, tp_rows)], in_sem.at[slot]
        ).wait()
    mixed_sent()


def solution(mesh):
    kv_n, tp_n = mesh.shape["kv"], mesh.shape["tp"]

    def per_device(*args):
        args = list(args)
        for place in (1, 7, 12):
            args[place] = args[place].reshape(1, -1)
        for place in (6, 10, 13, 14):
            args[place] = args[place].T
        tokens, w_query, w_value, state_c, w_gateff = (args[i] for i in (0, 2, 4, 8, 13))
        batch, width = tokens.shape
        rows, tp_rows = batch // kv_n, batch // tp_n
        value_size, query_size = state_c.shape[2:]
        ff = w_gateff.shape[0]
        ff_pad = up_to_lanes(ff)
        proj_width = 2 * query_size + 2 * value_size
        heads_all = args[7].shape[1]
        V = pltpu.VMEM
        scratch = [
            V((batch, width), bf16),
            V((1, width), f32),
            V((width, proj_width), bf16),
            V((2 * heads_all, width), bf16),
            V((1, heads_all), f32),
            V((rows, value_size, query_size), f32),
            V((rows, 1, query_size), f32),
            V((1, rows), f32),
            V((value_size, width), bf16),
            V((1, width), f32),
            V((ff, width), bf16),
            V((ff, width), bf16),
            V((ff, width), bf16),
            V((rows, value_size, query_size), bf16),
            V((rows, value_size, query_size), f32),
            V((rows, 1, query_size), f32),
            V((1, rows), f32),
            V((kv_n, rows, proj_width + LANES), bf16),
            V((kv_n, rows, proj_width + LANES), bf16),
            V((kv_n, rows, value_size), bf16),
            V((tp_n, tp_rows, width), bf16),
            V((tp_n, tp_rows, width), bf16),
            V((tp_n, tp_rows, width), bf16),
            V((kv_n, rows, 2 * ff_pad + LANES), bf16),
            V((kv_n, rows, 2 * ff_pad + LANES), bf16),
            V((kv_n, rows, ff), bf16),
            V((tp_n, tp_rows, width), bf16),
            V((tp_n, tp_rows, width), bf16),
            V((tp_n, tp_rows, width), bf16),
            pltpu.SemaphoreType.DMA((16,)),
            pltpu.SemaphoreType.DMA((2 + rows,)),
            pltpu.SemaphoreType.DMA((4, kv_n)),
            pltpu.SemaphoreType.DMA((4, kv_n)),
            pltpu.SemaphoreType.DMA((4, tp_n)),
            pltpu.SemaphoreType.DMA((4, tp_n)),
        ]
        anywhere = pl.BlockSpec(memory_space=pl.ANY)
        outs = pl.pallas_call(
            functools.partial(layer, kv_n, tp_n),
            out_shape=(
                jax.ShapeDtypeStruct((batch, width), bf16),
                jax.ShapeDtypeStruct(state_c.shape, f32),
                jax.ShapeDtypeStruct(args[9].shape, f32),
                jax.ShapeDtypeStruct(args[10].shape, f32),
            ),
            in_specs=[anywhere] * len(args),
            out_specs=(anywhere,) * 4,
            scratch_shapes=scratch,
            compiler_params=pltpu.CompilerParams(
                collective_id=0, has_side_effects=True, vmem_limit_bytes=60 * 1024 * 1024
            ),
        )(*args)
        return (*outs[:3], outs[3].T)

    placed = (
        P(None, "kv"),
        P("kv"),
        P("kv", "tp"),
        P("kv", "tp"),
        P("kv", "tp"),
        P("kv", "tp"),
        P(),
        P(),
        P("kv", "tp", None, None),
        P("kv", "tp", None),
        P("kv", "tp"),
        P("tp", "kv"),
        P("kv"),
        P("kv", "tp"),
        P("kv", "tp"),
        P("tp", "kv"),
    )
    return jax.shard_map(
        per_device,
        mesh=mesh,
        in_specs=placed,
        out_specs=(P(None, "kv"), P("kv", "tp", None, None), P("kv", "tp", None), P("kv", "tp")),
        check_vma=False,
    )
```

time: 152 us -> 66.7 us (0.44)
  Pallas kernels: 0 us -> 58.8 us
  waiting for transfers between devices: 48.4 us -> 0 us
  blocking collectives: 38.8 us -> 0 us
  starting transfers between devices: 38.1 us -> 0 us
  matrix products: 7.97 us -> 0 us
  other arithmetic: 6.94 us -> 0 us
  local copies, waits for them, and re-layouts: 9.79 us -> 7.1 us
    pallas_call x0 -> x1, Pallas kernels: none -> 58.8 us  [per_device(): pl.pallas_call(functools.partial(layer, kv_n, tp_n), out_shape=(jax.Shape...]
    all_to_all x7 -> x0, waiting for transfers between devices: 48.4 us -> none  [the longest x6 34 us: sum_at_owner(): lax.all_to_all(pieces, axis, split_axis=0, concat_axis=0, tiled=True)]
    all_to_all x3 -> x0, blocking collectives: 38.8 us -> none  [sent_to_all(): return lax.all_to_all(copies, axis, split_axis=0, concat_axis=0, tiled=True)]
    all_to_all x7 -> x0, starting transfers between devices: 38.1 us -> none  [the longest x6 28.9 us: sum_at_owner(): lax.all_to_all(pieces, axis, split_axis=0, concat_axis=0, tiled=True)]
    dot_general x7 -> x0, matrix products: 7.97 us -> none  [the longest x1 3.63 us: per_device(): jnp.einsum('bhvd,bhd->bhv', new_c, query, precision=lax.Precision.HIGHEST)]
    convert_element_type x5 -> x0, local copies, waits for them, and re-layouts: 3.98 us -> none  [short(): return part.astype(jnp.bfloat16) if part.dtype == jnp.float32 else part]
    unnamed x18 -> x8, local copies, waits for them, and re-layouts: 3.33 us -> 7.1 us
    add x1 -> x0, other arithmetic: 2.6 us -> none  [per_device(): keep[:, :, None, None] * state_c]
  transfers between devices with their start and end apart: 7 -> 0, of which waited for: 7 -> 0; matrix products, arithmetic and copies ran while one was open for 7% -> 0% of each run, Pallas kernels for 0% -> 0%
where the time goes in v1:
time: 66.7 us; the launch traced here: 66.5 us
  Pallas kernels  58.8 us (88%)
  local copies, waits for them, and re-layouts  7.1 us (11%)
    pallas_call x1, Pallas kernels, per_device(): pl.pallas_call(functools.partial(layer, kv_n, tp_n), out_shape=(jax.Shape...  58.8 us
    unnamed x8, local copies, waits for them, and re-layouts  7.1 us

profile of v1, /device:TPU:1, one launch (start us, length us, event | category | flops | bytes accessed | tf_op | source)
XLA Modules:
  0.0 66.5 jit_solution(18133726622099495425)
XLA Ops:
  0.6 58.8 %shard_map.183 = (bf16[128,256]{1,0:T(8,128)(2,1)}, f32[8,1,512,256]{3,2,1,0:T(8,128)}, f32[8,1,256]{2,1,0:T(1,128)}, f32[1,8]{1,0:T(1,128)}) custom-call(bf16[128,256]{1,0:T(8,128)(2,1)} %tokens.1, f32[1,256]{1,0:T(1,128)} %bitcast.11, bf16[256,256]{1,0:T(8,128)(2,1)} %w_query.1, bf16[256,256]{1,0:T(8,128)(2,1)} %w_key.1, bf16[256,512]{1,0:T(8,128)(2,1)} %w_value.1, ...), custom_call_target="tpu_custom_call" | custom-call | tf_op jit(solution)/shard_map/pallas_call | solution.py:413
  59.4 1.5 %copy.24 = bf16[128,256]{1,0:T(8,128)(2,1)} copy(bf16[128,256]{1,0:T(8,128)(2,1)} %get-tuple-element.16) | data formatting | bytes 131072
  60.9 0.0 copy-start
  60.9 0.0 copy-start.1
  60.9 4.5 %copy.25 = f32[8,1,512,256]{3,2,1,0:T(8,128)} copy(f32[8,1,512,256]{3,2,1,0:T(8,128)} %get-tuple-element.17) | data formatting | bytes 8388608
  65.4 0.0 copy-done
  65.4 0.6 copy.26
  66.0 0.0 copy-done.1
  66.0 0.5 copy.27
Async XLA Ops:
  60.9 4.5 %copy-start = (f32[8,1,256]{2,1,0:T(1,128)S(1)}, f32[8,1,256]{2,1,0:T(1,128)}, u32[]{:S(2)}) copy-start(f32[8,1,256]{2,1,0:T(1,128)} %get-tuple-element.18) | copy-start | bytes 24580
  60.9 5.1 %copy-start.1 = (f32[1,8]{1,0:T(1,128)S(1)}, f32[1,8]{1,0:T(1,128)}, u32[]{:S(2)}) copy-start(f32[1,8]{1,0:T(1,128)} %get-tuple-element.11) | copy-start | bytes 100

commit v2 on v1

--- a/solution.py
+++ b/solution.py
@@ -67,9 +67,6 @@
     w_upff_v,
     w_down_v,
     c_short,
-    c_new,
-    n_new,
-    m_new,
     proj_send,
     proj_recv,
     head_all,
@@ -81,9 +78,7 @@
     hidden_all,
     down_send,
     down_recv,
-    mixed_all,
     in_sem,
-    out_sem,
     kv_send_sem,
     kv_recv_sem,
     tp_send_sem,
@@ -101,6 +96,37 @@
     ff = w_gateff_v.shape[0]
     ff_pad = up_to_lanes(ff)
 
+    near = {0: 0, 1: 1, 2: 2, 3: 1}
+    side = 4
+
+    def peer_at(axis, offset):
+        first, second = offset
+        if axis == "kv":
+            return lax.rem(kv // side + first, side) * side + lax.rem(kv % side + second, side)
+        return lax.rem(tp // 2 + first, side) * 2 + lax.rem(tp % 2 + second, 2)
+
+    kv_order = [(a, b) for a in range(side) for b in range(side) if a or b]
+    kv_order.sort(key=lambda offset: -near[offset[0]] - near[offset[1]])
+    tp_order = [(a, b) for a in range(side) for b in range(2) if a or b]
+    tp_order.sort(key=lambda offset: -near[offset[0]])
+
+    barrier = pltpu.get_barrier_semaphore()
+
+    def greet_kv(step, carry):
+        pl.semaphore_signal(
+            barrier, inc=1, device_id={"kv": lax.rem(kv + step, kv_n)}, device_id_type=MESH
+        )
+        return carry
+
+    def greet_tp(step, carry):
+        pl.semaphore_signal(
+            barrier, inc=1, device_id={"tp": lax.rem(tp + step, tp_n)}, device_id_type=MESH
+        )
+        return carry
+
+    lax.fori_loop(1, kv_n, greet_kv, 0)
+    lax.fori_loop(1, tp_n, greet_tp, 0)
+
     loads = []
 
     def load(source, target):
@@ -122,23 +148,6 @@
     load_ff = [load(mlp_gain, gain_two_v), load(w_gateff, w_gateff_v), load(w_upff, w_upff_v)]
     load_down = load(w_downff, w_down_v)
 
-    barrier = pltpu.get_barrier_semaphore()
-
-    def greet_kv(step, carry):
-        pl.semaphore_signal(
-            barrier, inc=1, device_id={"kv": lax.rem(kv + step, kv_n)}, device_id_type=MESH
-        )
-        return carry
-
-    def greet_tp(step, carry):
-        pl.semaphore_signal(
-            barrier, inc=1, device_id={"tp": lax.rem(tp + step, tp_n)}, device_id_type=MESH
-        )
-        return carry
-
-    lax.fori_loop(1, kv_n, greet_kv, 0)
-    lax.fori_loop(1, tp_n, greet_tp, 0)
-
     def exchange(axis, phase, source_of, target):
         me, count = (kv, kv_n) if axis == "kv" else (tp, tp_n)
         sends, recvs = (kv_send_sem, kv_recv_sem) if axis == "kv" else (tp_send_sem, tp_recv_sem)
@@ -163,11 +172,9 @@
                 device_id_type=MESH,
             )
 
-        def start(step, carry):
-            copy_to(lax.rem(me + step, count)).start()
-            return carry
-
-        lax.fori_loop(1, count, start, 0)
+        order = kv_order if axis == "kv" else tp_order
+        for offset in order:
+            copy_to(peer_at(axis, offset)).start()
 
         def arrived(step):
             peer = lax.rem(me + step, count)
@@ -274,23 +281,14 @@
     head_all[kv] = (jax.nn.sigmoid(out_pre) * numer / denom).astype(bf16)
     head_arrived, _, head_sent = exchange("kv", 1, lambda peer: head_all.at[kv], head_all)
 
-    n_new[:, 0, :] = n_next
-    m_new[...] = jnp.sum(jnp.where(same, m_next, 0.0), axis=0, keepdims=True)
-    stores = [
-        pltpu.make_async_copy(n_new, new_n, out_sem.at[0]),
-        pltpu.make_async_copy(m_new, new_m, out_sem.at[1]),
-    ]
-    for copy in stores:
-        copy.start()
+    new_n[:, 0, :] = n_next
+    new_m[...] = jnp.sum(jnp.where(same, m_next, 0.0), axis=0, keepdims=True)
     admitted_column = admitted.T
     for one in range(rows):
-        c_new[one] = (
+        new_c[one, 0] = (
             keep[one : one + 1, :] * c_v[one]
             + admitted_column[:, one : one + 1] * key_vec[one : one + 1, :]
         )
-        copy = pltpu.make_async_copy(c_new.at[one], new_c.at[one, 0], out_sem.at[2 + one])
-        copy.start()
-        stores.append(copy)
 
     load_out.wait()
     head_arrived()
@@ -336,22 +334,24 @@
     down_send[...] = down_part.reshape(tp_n, tp_rows, width).astype(bf16)
     _, down_total, down_sent = exchange("tp", 2, lambda peer: down_send.at[peer], down_recv)
     down_sum = down_total(down_send[tp].astype(f32))
-    mixed_all[tp] = (mid_all[tp].astype(f32) + down_sum).astype(bf16)
-    mixed_arrived, _, mixed_sent = exchange("tp", 3, lambda peer: mixed_all.at[tp], mixed_all)
+    mixed[tp] = (mid_all[tp].astype(f32) + down_sum).astype(bf16)
+    mixed_arrived, _, mixed_sent = exchange("tp", 3, lambda peer: mixed.at[tp], mixed)
     for sent in (proj_sent, head_sent, attn_sent, mid_sent, ff_sent, hidden_sent, down_sent):
         sent()
-    for copy in stores:
+    mixed_arrived()
+    mixed_sent()
+
+
+def write_out(count, *refs):
+    sources, targets, sem = refs[:count], refs[count : 2 * count], refs[-1]
+    copies = [
+        pltpu.make_async_copy(source, target, sem.at[place])
+        for place, (source, target) in enumerate(zip(sources, targets))
+    ]
+    for copy in copies:
+        copy.start()
+    for copy in copies:
         copy.wait()
-    mixed_arrived()
-    for slot in range(tp_n):
-        pltpu.make_async_copy(
-            mixed_all.at[slot], mixed.at[pl.ds(slot * tp_rows, tp_rows)], in_sem.at[slot]
-        ).start()
-    for slot in range(tp_n):
-        pltpu.make_async_copy(
-            mixed_all.at[slot], mixed.at[pl.ds(slot * tp_rows, tp_rows)], in_sem.at[slot]
-        ).wait()
-    mixed_sent()
 
 
 def solution(mesh):
@@ -387,9 +387,6 @@
             V((ff, width), bf16),
             V((ff, width), bf16),
             V((rows, value_size, query_size), bf16),
-            V((rows, value_size, query_size), f32),
-            V((rows, 1, query_size), f32),
-            V((1, rows), f32),
             V((kv_n, rows, proj_width + LANES), bf16),
             V((kv_n, rows, proj_width + LANES), bf16),
             V((kv_n, rows, value_size), bf16),
@@ -401,31 +398,39 @@
             V((kv_n, rows, ff), bf16),
             V((tp_n, tp_rows, width), bf16),
             V((tp_n, tp_rows, width), bf16),
-            V((tp_n, tp_rows, width), bf16),
             pltpu.SemaphoreType.DMA((16,)),
-            pltpu.SemaphoreType.DMA((2 + rows,)),
             pltpu.SemaphoreType.DMA((4, kv_n)),
             pltpu.SemaphoreType.DMA((4, kv_n)),
             pltpu.SemaphoreType.DMA((4, tp_n)),
             pltpu.SemaphoreType.DMA((4, tp_n)),
         ]
         anywhere = pl.BlockSpec(memory_space=pl.ANY)
+        inside = pl.BlockSpec(memory_space=pltpu.VMEM)
+        results = (
+            ((tp_n, tp_rows, width), bf16),
+            (state_c.shape, f32),
+            (args[9].shape, f32),
+            (args[10].shape, f32),
+        )
         outs = pl.pallas_call(
             functools.partial(layer, kv_n, tp_n),
-            out_shape=(
-                jax.ShapeDtypeStruct((batch, width), bf16),
-                jax.ShapeDtypeStruct(state_c.shape, f32),
-                jax.ShapeDtypeStruct(args[9].shape, f32),
-                jax.ShapeDtypeStruct(args[10].shape, f32),
-            ),
+            out_shape=tuple(V(shape, dtype) for shape, dtype in results),
             in_specs=[anywhere] * len(args),
-            out_specs=(anywhere,) * 4,
+            out_specs=(inside,) * 4,
             scratch_shapes=scratch,
             compiler_params=pltpu.CompilerParams(
-                collective_id=0, has_side_effects=True, vmem_limit_bytes=60 * 1024 * 1024
+                collective_id=0, has_side_effects=True, vmem_limit_bytes=58 * 1024 * 1024
             ),
         )(*args)
-        return (*outs[:3], outs[3].T)
+        outs = pl.pallas_call(
+            functools.partial(write_out, len(outs)),
+            out_shape=tuple(jax.ShapeDtypeStruct(shape, dtype) for shape, dtype in results),
+            in_specs=[inside] * len(outs),
+            out_specs=(anywhere,) * len(outs),
+            scratch_shapes=[pltpu.SemaphoreType.DMA((len(outs),))],
+            compiler_params=pltpu.CompilerParams(vmem_limit_bytes=1024 * 1024),
+        )(*outs)
+        return (outs[0].reshape(batch, width), outs[1], outs[2], outs[3].T)
 
     placed = (
         P(None, "kv"),

time: 66.7 us -> 58.3 us (0.87)
  local copies, waits for them, and re-layouts: 7.1 us -> 0 us
  Pallas kernels: 58.8 us -> 57.6 us
    unnamed x8 -> x0, local copies, waits for them, and re-layouts: 7.1 us -> none
    pallas_call x1 -> x2, Pallas kernels: 58.8 us -> 57.6 us  [the longest x1 55.5 us: per_device(): pl.pallas_call(functools.partial(layer, kv_n, tp_n), out_shape=tuple((V(s...]
where the time goes in v2:
time: 58.3 us; the launch traced here: 58.2 us
  Pallas kernels  57.6 us (99%)
  between operations  0.65 us (1%)
    pallas_call x1, Pallas kernels, per_device(): pl.pallas_call(functools.partial(layer, kv_n, tp_n), out_shape=tuple((V(s...  55.5 us
    pallas_call x1, Pallas kernels, per_device(): pl.pallas_call(functools.partial(write_out, len(outs)), out_shape=tuple((...  2.08 us

profile of v2, /device:TPU:1, one launch (start us, length us, event | category | flops | bytes accessed | tf_op | source)
XLA Modules:
  0.0 58.2 jit_solution(2741904244278718861)
XLA Ops:
  0.6 55.5 %shard_map.183 = (bf16[8,16,256]{2,1,0:T(8,128)(2,1)S(1)}, f32[8,1,512,256]{3,2,1,0:T(8,128)S(1)}, f32[8,1,256]{2,1,0:T(1,128)S(1)}, f32[1,8]{1,0:T(1,128)S(1)}) custom-call(bf16[128,256]{1,0:T(8,128)(2,1)} %tokens.1, f32[1,256]{1,0:T(1,128)} %bitcast.12, bf16[256,256]{1,0:T(8,128)(2,1)} %w_query.1, bf16[256,256]{1,0:T(8,128)(2,1)} %w_key.1, ...), custom_call_target="tpu_custom_call" | custom-call | tf_op jit(solution)/shard_map/pallas_call | solution.py:415
  56.2 2.1 %shard_map.184 = (bf16[8,16,256]{2,1,0:T(8,128)(2,1)}, f32[8,1,512,256]{3,2,1,0:T(8,128)}, f32[8,1,256]{2,1,0:T(1,128)}, f32[1,8]{1,0:T(1,128)}) custom-call(bf16[8,16,256]{2,1,0:T(8,128)(2,1)S(1)} %get-tuple-element.12.refs_0_, f32[8,1,512,256]{3,2,1,0:T(8,128)S(1)} %get-tuple-element.13.refs_1_, f32[8,1,256]{2,1,0:T(1,128)S(1)} %get-tuple-element.14.refs_2_, ...), custom_call_target="tpu_custom_call" | custom-call | tf_op jit(solution)/shard_map/pallas_call | solution.py:425

commit v3 on v2

--- a/solution.py
+++ b/solution.py
@@ -86,9 +86,8 @@
 ):
     kv = lax.axis_index("kv")
     tp = lax.axis_index("tp")
-    batch, width = tok_v.shape
-    rows = batch // kv_n
-    tp_rows = batch // tp_n
+    _, rows, width = tok_v.shape
+    batch = kv_n * rows
     width_all = width * kv_n
     heads_all = bias_v.shape[1]
     value_size, query_size = c_v.shape[1:]
@@ -96,19 +95,31 @@
     ff = w_gateff_v.shape[0]
     ff_pad = up_to_lanes(ff)
 
+    side = 4
     near = {0: 0, 1: 1, 2: 2, 3: 1}
-    side = 4
-
-    def peer_at(axis, offset):
-        first, second = offset
-        if axis == "kv":
-            return lax.rem(kv // side + first, side) * side + lax.rem(kv % side + second, side)
-        return lax.rem(tp // 2 + first, side) * 2 + lax.rem(tp % 2 + second, 2)
-
-    kv_order = [(a, b) for a in range(side) for b in range(side) if a or b]
-    kv_order.sort(key=lambda offset: -near[offset[0]] - near[offset[1]])
-    tp_order = [(a, b) for a in range(side) for b in range(2) if a or b]
-    tp_order.sort(key=lambda offset: -near[offset[0]])
+    kv_z, kv_y = kv // side, lax.rem(kv, side)
+    tp_x, tp_core = tp // 2, lax.rem(tp, 2)
+
+    def far_first(offsets):
+        return sorted(offsets, key=lambda offset: -near[offset[0]] - near[offset[1]])
+
+    square = [(a, b) for a in range(side) for b in range(side)]
+    even = far_first([offset for offset in square if sum(offset) % 2 == 0])
+    odd = far_first([offset for offset in square if sum(offset) % 2 == 1])
+    around = far_first([offset for offset in square if offset != (0, 0)])
+    tp_around = sorted([(a, b) for a in range(side) for b in range(2) if a or b], key=lambda at: -near[at[0]])
+
+    def kv_peer(first, second):
+        return lax.rem(kv_z + first, side) * side + lax.rem(kv_y + second, side)
+
+    def tp_peer(first, second):
+        return lax.rem(tp_x + first, side) * 2 + lax.rem(tp_core + second, 2)
+
+    def block(group, place):
+        first = place // 2
+        return first * side + 2 * (place % 2) + (first + group) % 2
+
+    parity = lax.rem(kv_z + kv_y, 2)
 
     barrier = pltpu.get_barrier_semaphore()
 
@@ -148,64 +159,113 @@
     load_ff = [load(mlp_gain, gain_two_v), load(w_gateff, w_gateff_v), load(w_upff, w_upff_v)]
     load_down = load(w_downff, w_down_v)
 
-    def exchange(axis, phase, source_of, target):
-        me, count = (kv, kv_n) if axis == "kv" else (tp, tp_n)
-        sends, recvs = (kv_send_sem, kv_recv_sem) if axis == "kv" else (tp_send_sem, tp_recv_sem)
-
-        def copy_to(peer):
-            return pltpu.make_async_remote_copy(
-                src_ref=source_of(peer),
-                dst_ref=target.at[me],
-                send_sem=sends.at[phase, peer],
-                recv_sem=recvs.at[phase, me],
-                device_id={axis: peer},
-                device_id_type=MESH,
+    def kv_copy(phase, source, target, peer, origin):
+        return pltpu.make_async_remote_copy(
+            src_ref=source,
+            dst_ref=target,
+            send_sem=kv_send_sem.at[phase, peer],
+            recv_sem=kv_recv_sem.at[phase, origin],
+            device_id={"kv": peer},
+            device_id_type=MESH,
+        )
+
+    def tp_copy(phase, source, target, peer, origin):
+        return pltpu.make_async_remote_copy(
+            src_ref=source,
+            dst_ref=target,
+            send_sem=tp_send_sem.at[phase, peer],
+            recv_sem=tp_recv_sem.at[phase, origin],
+            device_id={"tp": peer},
+            device_id_type=MESH,
+        )
+
+    unsent = []
+
+    def scatter_group(phase, group, send, recv):
+        mine = lax.rem(parity + group, 2) == 0
+        for at_even, at_odd in zip(even, odd):
+            peer = kv_peer(
+                jnp.where(mine, at_even[0], at_odd[0]), jnp.where(mine, at_even[1], at_odd[1])
             )
-
-        def copy_from(peer):
-            return pltpu.make_async_remote_copy(
-                src_ref=source_of(peer),
-                dst_ref=target.at[peer],
-                send_sem=sends.at[phase, peer],
-                recv_sem=recvs.at[phase, peer],
-                device_id={axis: peer},
-                device_id_type=MESH,
-            )
-
-        order = kv_order if axis == "kv" else tp_order
-        for offset in order:
-            copy_to(peer_at(axis, offset)).start()
-
-        def arrived(step):
-            peer = lax.rem(me + step, count)
-            copy_from(peer).wait_recv()
-            return peer
-
-        def all_arrived():
-            def wait(step, carry):
-                arrived(step)
-                return carry
-
-            lax.fori_loop(1, count, wait, 0)
-
-        def sent():
-            def wait(step, carry):
-                copy_to(lax.rem(me + step, count)).wait_send()
-                return carry
-
-            lax.fori_loop(1, count, wait, 0)
-
-        def total(own):
-            def add(step, carry):
-                return carry + target[arrived(step)].astype(f32)
-
-            return lax.fori_loop(1, count, add, own)
-
-        return all_arrived, total, sent
+            copy = kv_copy(phase, send.at[peer], recv.at[kv], peer, kv)
+            if at_even == (0, 0):
+                pl.when(jnp.logical_not(mine))(copy.start)
+            else:
+                copy.start()
+
+    def scatter_total(phase, send, recv):
+        def add(step, carry):
+            peer = lax.rem(kv + step, kv_n)
+            kv_copy(phase, send.at[peer], recv.at[peer], peer, peer).wait_recv()
+            return carry + recv[peer].astype(f32)
+
+        def sent(step, carry):
+            peer = lax.rem(kv + step, kv_n)
+            kv_copy(phase, send.at[peer], recv.at[kv], peer, kv).wait_send()
+            return carry
+
+        unsent.append((kv_n, sent))
+        return lax.fori_loop(1, kv_n, add, send[kv].astype(f32))
+
+    def gather_start(phase, blocks):
+        for offset in around:
+            peer = kv_peer(*offset)
+            kv_copy(phase, blocks.at[kv], blocks.at[kv], peer, kv).start()
+
+        def sent(step, carry):
+            peer = lax.rem(kv + step, kv_n)
+            kv_copy(phase, blocks.at[kv], blocks.at[kv], peer, kv).wait_send()
+            return carry
+
+        unsent.append((kv_n, sent))
+
+    def gathered(phase, group, blocks):
+        for place in range(tp_n):
+            peer = block(group, place)
+            copy = kv_copy(phase, blocks.at[peer], blocks.at[peer], peer, peer)
+            pl.when(kv != peer)(copy.wait_recv)
+        parts = [blocks[block(group, place)].astype(f32) for place in range(tp_n)]
+        return jnp.concatenate(parts, axis=0).astype(bf16)
+
+    def tp_sent(phase, source_of, target):
+        def sent(step, carry):
+            peer = lax.rem(tp + step, tp_n)
+            tp_copy(phase, source_of(peer), target, peer, tp).wait_send()
+            return carry
+
+        unsent.append((tp_n, sent))
+
+    def sum_start(phase, group, part, send, recv):
+        for place in range(tp_n):
+            send[block(group, place)] = part[place * rows : (place + 1) * rows].astype(bf16)
+        for offset in tp_around:
+            peer = tp_peer(*offset)
+            tp_copy(phase, send.at[block(group, peer)], recv.at[group, tp], peer, tp).start()
+        tp_sent(phase, lambda peer: send.at[block(group, peer)], recv.at[group, tp])
+
+    def sum_total(phase, group, send, recv):
+        total = send[block(group, tp)].astype(f32)
+        for offset in reversed(tp_around):
+            peer = tp_peer(*offset)
+            tp_copy(phase, send.at[block(group, tp)], recv.at[group, peer], peer, peer).wait_recv()
+            total = total + recv[group, peer].astype(f32)
+        return total
+
+    def share_start(phase, group, blocks):
+        at = blocks.at[block(group, tp)]
+        for offset in tp_around:
+            tp_copy(phase, at, at, tp_peer(*offset), tp).start()
+        tp_sent(phase, lambda peer: at, at)
+
+    def shared(phase, group, blocks):
+        for offset in reversed(tp_around):
+            peer = tp_peer(*offset)
+            at = blocks.at[block(group, peer)]
+            tp_copy(phase, at, at, peer, peer).wait_recv()
 
     for copy in first:
         copy.wait()
-    tok_float = tok_v[...].astype(f32)
+    tok_float = tok_v[...].astype(f32).reshape(batch, width)
     squares_one = jnp.sum(tok_float * tok_float, axis=1, keepdims=True)
     normed_one = (tok_float * gain_one_v[...]).astype(bf16)
     lanes = lane_ids(batch)
@@ -229,7 +289,8 @@
         proj_send[:, :, pl.ds(at, step)] = part.reshape(kv_n, rows, step).astype(bf16)
 
     pl.semaphore_wait(barrier, kv_n + tp_n - 2)
-    _, proj_total, proj_sent = exchange("kv", 0, lambda peer: proj_send.at[peer], proj_recv)
+    for group in range(2):
+        scatter_group(0, group, proj_send, proj_recv)
 
     load_c.wait()
     for one in range(rows):
@@ -237,7 +298,7 @@
     for copy in load_cell:
         copy.wait()
 
-    proj_rows = proj_total(proj_send[kv].astype(f32))
+    proj_rows = scatter_total(0, proj_send, proj_recv)
     extra = proj_rows[:, proj_width:]
     lanes = lane_ids(rows)
 
@@ -279,7 +340,7 @@
     admitted = admit * value
     numer = keep * read + admitted * key_query
     head_all[kv] = (jax.nn.sigmoid(out_pre) * numer / denom).astype(bf16)
-    head_arrived, _, head_sent = exchange("kv", 1, lambda peer: head_all.at[kv], head_all)
+    gather_start(1, head_all)
 
     new_n[:, 0, :] = n_next
     new_m[...] = jnp.sum(jnp.where(same, m_next, 0.0), axis=0, keepdims=True)
@@ -291,55 +352,62 @@
         )
 
     load_out.wait()
-    head_arrived()
-    heads = head_all[...].astype(f32).reshape(batch, value_size).astype(bf16)
-    attn_part = dot(heads, w_out_v[...])
-    attn_send[...] = attn_part.reshape(tp_n, tp_rows, width).astype(bf16)
-    _, attn_total, attn_sent = exchange("tp", 0, lambda peer: attn_send.at[peer], attn_recv)
-    own_rows = pl.ds(pl.multiple_of(tp * tp_rows, tp_rows), tp_rows)
-    attn_mix = attn_total(attn_send[tp].astype(f32))
-    mid_all[tp] = (tok_v[own_rows, :].astype(f32) + attn_mix).astype(bf16)
-    mid_arrived, _, mid_sent = exchange("tp", 1, lambda peer: mid_all.at[tp], mid_all)
+    for group in range(2):
+        heads = gathered(1, group, head_all)
+        sum_start(group, group, dot(heads, w_out_v[...]), attn_send, attn_recv)
+    for group in range(2):
+        own = block(group, tp)
+        attn_mix = sum_total(group, group, attn_send, attn_recv)
+        mid_all[own] = (tok_v[own].astype(f32) + attn_mix).astype(bf16)
+        share_start(2 + group, group, mid_all)
     for copy in load_ff:
         copy.wait()
-    mid_arrived()
-
-    mid_float = mid_all[...].astype(f32).reshape(batch, width)
-    squares_two = jnp.sum(mid_float * mid_float, axis=1, keepdims=True)
-    normed_two = (mid_float * gain_two_v[...]).astype(bf16)
-    lanes = lane_ids(batch)
-    squares_short = squares_two.astype(bf16).astype(f32)
-    extra = jnp.where(
-        lanes == 0, squares_short, jnp.where(lanes == 1, squares_two - squares_short, 0.0)
-    )
-    ff_send[:, :, pl.ds(2 * ff_pad, LANES)] = extra.reshape(kv_n, rows, LANES).astype(bf16)
-    for base, weight in ((0, w_gateff_v), (ff_pad, w_upff_v)):
-        for at in range(0, ff, step):
-            columns = min(step, ff - at)
-            part = dot_rows(normed_two, weight[pl.ds(at, columns), :])
-            ff_send[:, :, pl.ds(base + at, columns)] = part.reshape(kv_n, rows, columns).astype(bf16)
-    _, ff_total, ff_sent = exchange("kv", 2, lambda peer: ff_send.at[peer], ff_recv)
-    ff_rows = ff_total(ff_send[kv].astype(f32))
+
+    for group in range(2):
+        shared(2 + group, group, mid_all)
+        parts = [mid_all[block(group, place)].astype(f32) for place in range(tp_n)]
+        mid_float = jnp.concatenate(parts, axis=0)
+        squares_two = jnp.sum(mid_float * mid_float, axis=1, keepdims=True)
+        normed_two = (mid_float * gain_two_v[...]).astype(bf16)
+        lanes = lane_ids(tp_n * rows)
+        squares_short = squares_two.astype(bf16).astype(f32)
+        extra = jnp.where(
+            lanes == 0, squares_short, jnp.where(lanes == 1, squares_two - squares_short, 0.0)
+        )
+        pieces = [(2 * ff_pad, LANES, extra)]
+        for base, weight in ((0, w_gateff_v), (ff_pad, w_upff_v)):
+            for at in range(0, ff, step):
+                columns = min(step, ff - at)
+                pieces.append(
+                    (base + at, columns, dot_rows(normed_two, weight[pl.ds(at, columns), :]))
+                )
+        for at, columns, part in pieces:
+            for place in range(tp_n):
+                ff_send[block(group, place), :, pl.ds(at, columns)] = part[
+                    place * rows : (place + 1) * rows
+                ].astype(bf16)
+        scatter_group(2, group, ff_send, ff_recv)
+    ff_rows = scatter_total(2, ff_send, ff_recv)
     rows_two = jnp.sum(ff_rows[:, 2 * ff_pad :], axis=1, keepdims=True)
     scale_two = lax.rsqrt(rows_two / width_all + norm_floor)
     gate_ff = ff_rows[:, :ff] * scale_two
     up_ff = ff_rows[:, ff_pad : ff_pad + ff] * scale_two
     hidden_all[kv] = (gate_ff / (1.0 + jnp.exp(-gate_ff)) * up_ff).astype(bf16)
-    hidden_arrived, _, hidden_sent = exchange("kv", 3, lambda peer: hidden_all.at[kv], hidden_all)
+    gather_start(3, hidden_all)
 
     load_down.wait()
-    hidden_arrived()
-    hidden = hidden_all[...].astype(f32).reshape(batch, ff).astype(bf16)
-    down_part = dot(hidden, w_down_v[...])
-    down_send[...] = down_part.reshape(tp_n, tp_rows, width).astype(bf16)
-    _, down_total, down_sent = exchange("tp", 2, lambda peer: down_send.at[peer], down_recv)
-    down_sum = down_total(down_send[tp].astype(f32))
-    mixed[tp] = (mid_all[tp].astype(f32) + down_sum).astype(bf16)
-    mixed_arrived, _, mixed_sent = exchange("tp", 3, lambda peer: mixed.at[tp], mixed)
-    for sent in (proj_sent, head_sent, attn_sent, mid_sent, ff_sent, hidden_sent, down_sent):
-        sent()
-    mixed_arrived()
-    mixed_sent()
+    for group in range(2):
+        hidden = gathered(3, group, hidden_all)
+        sum_start(4 + group, group, dot(hidden, w_down_v[...]), down_send, down_recv)
+    for group in range(2):
+        own = block(group, tp)
+        down_sum = sum_total(4 + group, group, down_send, down_recv)
+        mixed[own] = (mid_all[own].astype(f32) + down_sum).astype(bf16)
+        share_start(6 + group, group, mixed)
+    for count, sent in unsent:
+        lax.fori_loop(1, count, sent, 0)
+    for group in range(2):
+        shared(6 + group, group, mixed)
 
 
 def write_out(count, *refs):
@@ -365,7 +433,8 @@
             args[place] = args[place].T
         tokens, w_query, w_value, state_c, w_gateff = (args[i] for i in (0, 2, 4, 8, 13))
         batch, width = tokens.shape
-        rows, tp_rows = batch // kv_n, batch // tp_n
+        rows = batch // kv_n
+        args[0] = tokens.reshape(kv_n, rows, width)
         value_size, query_size = state_c.shape[2:]
         ff = w_gateff.shape[0]
         ff_pad = up_to_lanes(ff)
@@ -373,7 +442,7 @@
         heads_all = args[7].shape[1]
         V = pltpu.VMEM
         scratch = [
-            V((batch, width), bf16),
+            V((kv_n, rows, width), bf16),
             V((1, width), f32),
             V((width, proj_width), bf16),
             V((2 * heads_all, width), bf16),
@@ -390,24 +459,24 @@
             V((kv_n, rows, proj_width + LANES), bf16),
             V((kv_n, rows, proj_width + LANES), bf16),
             V((kv_n, rows, value_size), bf16),
-            V((tp_n, tp_rows, width), bf16),
-            V((tp_n, tp_rows, width), bf16),
-            V((tp_n, tp_rows, width), bf16),
+            V((kv_n, rows, width), bf16),
+            V((2, tp_n, rows, width), bf16),
+            V((kv_n, rows, width), bf16),
             V((kv_n, rows, 2 * ff_pad + LANES), bf16),
             V((kv_n, rows, 2 * ff_pad + LANES), bf16),
             V((kv_n, rows, ff), bf16),
-            V((tp_n, tp_rows, width), bf16),
-            V((tp_n, tp_rows, width), bf16),
+            V((kv_n, rows, width), bf16),
+            V((2, tp_n, rows, width), bf16),
             pltpu.SemaphoreType.DMA((16,)),
             pltpu.SemaphoreType.DMA((4, kv_n)),
             pltpu.SemaphoreType.DMA((4, kv_n)),
-            pltpu.SemaphoreType.DMA((4, tp_n)),
-            pltpu.SemaphoreType.DMA((4, tp_n)),
+            pltpu.SemaphoreType.DMA((8, tp_n)),
+            pltpu.SemaphoreType.DMA((8, tp_n)),
         ]
         anywhere = pl.BlockSpec(memory_space=pl.ANY)
         inside = pl.BlockSpec(memory_space=pltpu.VMEM)
         results = (
-            ((tp_n, tp_rows, width), bf16),
+            ((kv_n, rows, width), bf16),
             (state_c.shape, f32),
             (args[9].shape, f32),
             (args[10].shape, f32),

time: 58.3 us -> 60 us (1.029)
  Pallas kernels: 57.6 us -> 59.3 us
    pallas_call x1, Pallas kernels: 55.5 us -> 57.2 us  [per_device(): pl.pallas_call(functools.partial(layer, kv_n, tp_n), out_shape=tuple((V(s...]
where the time goes in v3:
time: 60 us; the launch traced here: 59.9 us
  Pallas kernels  59.3 us (99%)
  between operations  0.65 us (1%)
    pallas_call x1, Pallas kernels, per_device(): pl.pallas_call(functools.partial(layer, kv_n, tp_n), out_shape=tuple((V(s...  57.2 us
    pallas_call x1, Pallas kernels, per_device(): pl.pallas_call(functools.partial(write_out, len(outs)), out_shape=tuple((...  2.08 us

profile of v3, /device:TPU:1, one launch (start us, length us, event | category | flops | bytes accessed | tf_op | source)
XLA Modules:
  0.0 59.9 jit_solution(3535373843643517570)
XLA Ops:
  0.6 57.2 %shard_map.183 = (bf16[16,8,256]{2,1,0:T(8,128)(2,1)S(1)}, f32[8,1,512,256]{3,2,1,0:T(8,128)S(1)}, f32[8,1,256]{2,1,0:T(1,128)S(1)}, f32[1,8]{1,0:T(1,128)S(1)}) custom-call(bf16[16,8,256]{2,1,0:T(8,128)(2,1)} %bitcast.13, f32[1,256]{1,0:T(1,128)} %bitcast.14, bf16[256,256]{1,0:T(8,128)(2,1)} %w_query.1, bf16[256,256]{1,0:T(8,128)(2,1)} %w_key.1, ...), custom_call_target="tpu_custom_call" | custom-call | tf_op jit(solution)/shard_map/pallas_call | solution.py:484
  57.8 2.1 %shard_map.184 = (bf16[16,8,256]{2,1,0:T(8,128)(2,1)}, f32[8,1,512,256]{3,2,1,0:T(8,128)}, f32[8,1,256]{2,1,0:T(1,128)}, f32[1,8]{1,0:T(1,128)}) custom-call(bf16[16,8,256]{2,1,0:T(8,128)(2,1)S(1)} %get-tuple-element.12.refs_0_, f32[8,1,512,256]{3,2,1,0:T(8,128)S(1)} %get-tuple-element.13.refs_1_, f32[8,1,256]{2,1,0:T(1,128)S(1)} %get-tuple-element.14.refs_2_, ...), custom_call_target="tpu_custom_call" | custom-call | tf_op jit(solution)/shard_map/pallas_call | solution.py:494

commit v4 on v3

--- a/solution.py
+++ b/solution.py
@@ -70,14 +70,17 @@
     proj_send,
     proj_recv,
     head_all,
-    attn_send,
-    attn_recv,
+    part_f32,
+    attn_swap,
+    attn_swapped,
+    attn_quads,
     mid_all,
     ff_send,
     ff_recv,
     hidden_all,
-    down_send,
-    down_recv,
+    down_swap,
+    down_swapped,
+    down_quads,
     in_sem,
     kv_send_sem,
     kv_recv_sem,
@@ -86,40 +89,25 @@
 ):
     kv = lax.axis_index("kv")
     tp = lax.axis_index("tp")
-    _, rows, width = tok_v.shape
-    batch = kv_n * rows
+    _, half, width = tok_v.shape
+    batch = 2 * half
+    rows = batch // kv_n
     width_all = width * kv_n
     heads_all = bias_v.shape[1]
     value_size, query_size = c_v.shape[1:]
     proj_width = w_proj_v.shape[1]
-    ff = w_gateff_v.shape[0]
-    ff_pad = up_to_lanes(ff)
+    ff, ff_pad = w_down_v.shape[0], w_gateff_v.shape[0]
 
     side = 4
     near = {0: 0, 1: 1, 2: 2, 3: 1}
     kv_z, kv_y = kv // side, lax.rem(kv, side)
-    tp_x, tp_core = tp // 2, lax.rem(tp, 2)
-
-    def far_first(offsets):
-        return sorted(offsets, key=lambda offset: -near[offset[0]] - near[offset[1]])
-
-    square = [(a, b) for a in range(side) for b in range(side)]
-    even = far_first([offset for offset in square if sum(offset) % 2 == 0])
-    odd = far_first([offset for offset in square if sum(offset) % 2 == 1])
-    around = far_first([offset for offset in square if offset != (0, 0)])
-    tp_around = sorted([(a, b) for a in range(side) for b in range(2) if a or b], key=lambda at: -near[at[0]])
+    ring, core = tp // 2, lax.rem(tp, 2)
+    partner = ring * 2 + (1 - core)
+    around = [(a, b) for a in range(side) for b in range(side) if a or b]
+    around.sort(key=lambda offset: -near[offset[0]] - near[offset[1]])
 
     def kv_peer(first, second):
         return lax.rem(kv_z + first, side) * side + lax.rem(kv_y + second, side)
-
-    def tp_peer(first, second):
-        return lax.rem(tp_x + first, side) * 2 + lax.rem(tp_core + second, 2)
-
-    def block(group, place):
-        first = place // 2
-        return first * side + 2 * (place % 2) + (first + group) % 2
-
-    parity = lax.rem(kv_z + kv_y, 2)
 
     barrier = pltpu.get_barrier_semaphore()
 
@@ -156,7 +144,7 @@
     load_c = load(state_c.at[:, 0], c_v)
     load_cell = [load(state_n, n_v), load(state_m, m_v), load(forget_bias, bias_v)]
     load_out = load(w_output, w_out_v)
-    load_ff = [load(mlp_gain, gain_two_v), load(w_gateff, w_gateff_v), load(w_upff, w_upff_v)]
+    load_ff = [load(mlp_gain, gain_two_v), load(w_gateff, w_gateff_v.at[pl.ds(0, ff)]), load(w_upff, w_upff_v.at[pl.ds(0, ff)])]
     load_down = load(w_downff, w_down_v)
 
     def kv_copy(phase, source, target, peer, origin):
@@ -169,29 +157,20 @@
             device_id_type=MESH,
         )
 
-    def tp_copy(phase, source, target, peer, origin):
-        return pltpu.make_async_remote_copy(
-            src_ref=source,
-            dst_ref=target,
-            send_sem=tp_send_sem.at[phase, peer],
-            recv_sem=tp_recv_sem.at[phase, origin],
-            device_id={"tp": peer},
-            device_id_type=MESH,
-        )
-
     unsent = []
 
-    def scatter_group(phase, group, send, recv):
-        mine = lax.rem(parity + group, 2) == 0
-        for at_even, at_odd in zip(even, odd):
-            peer = kv_peer(
-                jnp.where(mine, at_even[0], at_odd[0]), jnp.where(mine, at_even[1], at_odd[1])
-            )
-            copy = kv_copy(phase, send.at[peer], recv.at[kv], peer, kv)
-            if at_even == (0, 0):
-                pl.when(jnp.logical_not(mine))(copy.start)
-            else:
-                copy.start()
+    def all_sent():
+        for wait in unsent:
+            wait()
+        unsent.clear()
+
+    def kv_sent(phase, source_of, target):
+        def one(step, carry):
+            peer = lax.rem(kv + step, kv_n)
+            kv_copy(phase, source_of(peer), target, peer, kv).wait_send()
+            return carry
+
+        unsent.append(lambda: lax.fori_loop(1, kv_n, one, 0))
 
     def scatter_total(phase, send, recv):
         def add(step, carry):
@@ -199,69 +178,64 @@
             kv_copy(phase, send.at[peer], recv.at[peer], peer, peer).wait_recv()
             return carry + recv[peer].astype(f32)
 
-        def sent(step, carry):
-            peer = lax.rem(kv + step, kv_n)
-            kv_copy(phase, send.at[peer], recv.at[kv], peer, kv).wait_send()
-            return carry
-
-        unsent.append((kv_n, sent))
+        kv_sent(phase, lambda peer: send.at[peer], recv.at[kv])
         return lax.fori_loop(1, kv_n, add, send[kv].astype(f32))
 
     def gather_start(phase, blocks):
         for offset in around:
             peer = kv_peer(*offset)
             kv_copy(phase, blocks.at[kv], blocks.at[kv], peer, kv).start()
-
-        def sent(step, carry):
+        kv_sent(phase, lambda peer: blocks.at[kv], blocks.at[kv])
+
+    def gathered(phase, blocks):
+        def wait(step, carry):
             peer = lax.rem(kv + step, kv_n)
-            kv_copy(phase, blocks.at[kv], blocks.at[kv], peer, kv).wait_send()
+            kv_copy(phase, blocks.at[peer], blocks.at[peer], peer, peer).wait_recv()
             return carry
 
-        unsent.append((kv_n, sent))
-
-    def gathered(phase, group, blocks):
-        for place in range(tp_n):
-            peer = block(group, place)
-            copy = kv_copy(phase, blocks.at[peer], blocks.at[peer], peer, peer)
-            pl.when(kv != peer)(copy.wait_recv)
-        parts = [blocks[block(group, place)].astype(f32) for place in range(tp_n)]
-        return jnp.concatenate(parts, axis=0).astype(bf16)
-
-    def tp_sent(phase, source_of, target):
-        def sent(step, carry):
-            peer = lax.rem(tp + step, tp_n)
-            tp_copy(phase, source_of(peer), target, peer, tp).wait_send()
-            return carry
-
-        unsent.append((tp_n, sent))
-
-    def sum_start(phase, group, part, send, recv):
-        for place in range(tp_n):
-            send[block(group, place)] = part[place * rows : (place + 1) * rows].astype(bf16)
-        for offset in tp_around:
-            peer = tp_peer(*offset)
-            tp_copy(phase, send.at[block(group, peer)], recv.at[group, tp], peer, tp).start()
-        tp_sent(phase, lambda peer: send.at[block(group, peer)], recv.at[group, tp])
-
-    def sum_total(phase, group, send, recv):
-        total = send[block(group, tp)].astype(f32)
-        for offset in reversed(tp_around):
-            peer = tp_peer(*offset)
-            tp_copy(phase, send.at[block(group, tp)], recv.at[group, peer], peer, peer).wait_recv()
-            total = total + recv[group, peer].astype(f32)
+        lax.fori_loop(1, kv_n, wait, 0)
+        return blocks[...].astype(f32).reshape(batch, blocks.shape[2]).astype(bf16)
+
+    def tp_copy(place, source, target, peer):
+        return pltpu.make_async_remote_copy(
+            src_ref=source,
+            dst_ref=target,
+            send_sem=tp_send_sem.at[place],
+            recv_sem=tp_recv_sem.at[place],
+            device_id={"tp": peer},
+            device_id_type=MESH,
+        )
+
+    def tp_total(first, part, part_f32, swap_send, swap_recv, quads):
+        part_f32[...] = part.reshape(2, half, width)
+        swap_send[...] = part_f32[1 - core].astype(bf16)
+        swap = tp_copy(first, swap_send, swap_recv, partner)
+        swap.start()
+        swap.wait_recv()
+        quads[ring] = (part_f32[core] + swap_recv[...].astype(f32)).astype(bf16)
+        copies = []
+        for offset in (2, 1, 3):
+            peer = lax.rem(ring + offset, side) * 2 + core
+            copies.append(tp_copy(first + offset, quads.at[ring], quads.at[ring], peer))
+        for copy in copies:
+            copy.start()
+        all_sent()
+        for offset in (3, 1, 2):
+            at = quads.at[lax.rem(ring + side - offset, side)]
+            tp_copy(first + offset, at, at, partner).wait_recv()
+        unsent.append(swap.wait_send)
+        unsent.extend(copy.wait_send for copy in copies)
+        total = quads[0].astype(f32)
+        for place in range(1, side):
+            total = total + quads[place].astype(f32)
         return total
 
-    def share_start(phase, group, blocks):
-        at = blocks.at[block(group, tp)]
-        for offset in tp_around:
-            tp_copy(phase, at, at, tp_peer(*offset), tp).start()
-        tp_sent(phase, lambda peer: at, at)
-
-    def shared(phase, group, blocks):
-        for offset in reversed(tp_around):
-            peer = tp_peer(*offset)
-            at = blocks.at[block(group, peer)]
-            tp_copy(phase, at, at, peer, peer).wait_recv()
+    def tp_share(place, halves):
+        copy = tp_copy(place, halves.at[core], halves.at[core], partner)
+        copy.start()
+        unsent.append(copy.wait_send)
+        other = halves.at[1 - core]
+        return tp_copy(place, other, other, partner).wait_recv
 
     for copy in first:
         copy.wait()
@@ -289,8 +263,9 @@
         proj_send[:, :, pl.ds(at, step)] = part.reshape(kv_n, rows, step).astype(bf16)
 
     pl.semaphore_wait(barrier, kv_n + tp_n - 2)
-    for group in range(2):
-        scatter_group(0, group, proj_send, proj_recv)
+    for offset in around:
+        peer = kv_peer(*offset)
+        kv_copy(0, proj_send.at[peer], proj_recv.at[kv], peer, kv).start()
 
     load_c.wait()
     for one in range(rows):
@@ -352,43 +327,43 @@
         )
 
     load_out.wait()
-    for group in range(2):
-        heads = gathered(1, group, head_all)
-        sum_start(group, group, dot(heads, w_out_v[...]), attn_send, attn_recv)
-    for group in range(2):
-        own = block(group, tp)
-        attn_mix = sum_total(group, group, attn_send, attn_recv)
-        mid_all[own] = (tok_v[own].astype(f32) + attn_mix).astype(bf16)
-        share_start(2 + group, group, mid_all)
+    heads = gathered(1, head_all)
+    attn_part = dot(heads, w_out_v[...])
+    attn_mix = tp_total(0, attn_part, part_f32, attn_swap, attn_swapped, attn_quads)
+    mid_all[core] = (tok_v[core].astype(f32) + attn_mix).astype(bf16)
+    mid_arrived = tp_share(4, mid_all)
     for copy in load_ff:
         copy.wait()
 
-    for group in range(2):
-        shared(2 + group, group, mid_all)
-        parts = [mid_all[block(group, place)].astype(f32) for place in range(tp_n)]
-        mid_float = jnp.concatenate(parts, axis=0)
+    lanes = lane_ids(half)
+    for turn in range(2):
+        at_half = core if turn == 0 else 1 - core
+        if turn == 1:
+            mid_arrived()
+        mid_float = mid_all[at_half].astype(f32)
         squares_two = jnp.sum(mid_float * mid_float, axis=1, keepdims=True)
         normed_two = (mid_float * gain_two_v[...]).astype(bf16)
-        lanes = lane_ids(tp_n * rows)
         squares_short = squares_two.astype(bf16).astype(f32)
-        extra = jnp.where(
-            lanes == 0, squares_short, jnp.where(lanes == 1, squares_two - squares_short, 0.0)
-        )
-        pieces = [(2 * ff_pad, LANES, extra)]
+        extra = jnp.where(lanes == LANES - 2, squares_short, squares_two - squares_short)
         for base, weight in ((0, w_gateff_v), (ff_pad, w_upff_v)):
-            for at in range(0, ff, step):
-                columns = min(step, ff - at)
-                pieces.append(
-                    (base + at, columns, dot_rows(normed_two, weight[pl.ds(at, columns), :]))
-                )
-        for at, columns, part in pieces:
-            for place in range(tp_n):
-                ff_send[block(group, place), :, pl.ds(at, columns)] = part[
-                    place * rows : (place + 1) * rows
-                ].astype(bf16)
-        scatter_group(2, group, ff_send, ff_recv)
+            for at in range(0, ff_pad, step):
+                columns = min(step, ff_pad - at)
+                part = dot_rows(normed_two, weight[pl.ds(at, columns), :])
+                if base == 0 and at + columns == ff_pad:
+                    last = jnp.where(lanes < LANES - 2, part[:, columns - LANES :], extra)
+                    part = jnp.concatenate([part[:, : columns - LANES], last], axis=1)
+                part = part.reshape(kv_n // 2, rows, columns).astype(bf16)
+                ff_send[pl.ds(at_half * (kv_n // 2), kv_n // 2), :, pl.ds(base + at, columns)] = part
+        for second in (2, 1, 3, 0):
+            for first in range(side // 2):
+                peer = (at_half * (side // 2) + first) * side + lax.rem(kv_y + second, side)
+                copy = kv_copy(2, ff_send.at[peer], ff_recv.at[kv], peer, kv)
+                if second == 0:
+                    pl.when(peer != kv)(copy.start)
+                else:
+                    copy.start()
     ff_rows = scatter_total(2, ff_send, ff_recv)
-    rows_two = jnp.sum(ff_rows[:, 2 * ff_pad :], axis=1, keepdims=True)
+    rows_two = jnp.sum(ff_rows[:, ff_pad - 2 : ff_pad], axis=1, keepdims=True)
     scale_two = lax.rsqrt(rows_two / width_all + norm_floor)
     gate_ff = ff_rows[:, :ff] * scale_two
     up_ff = ff_rows[:, ff_pad : ff_pad + ff] * scale_two
@@ -396,25 +371,23 @@
     gather_start(3, hidden_all)
 
     load_down.wait()
-    for group in range(2):
-        hidden = gathered(3, group, hidden_all)
-        sum_start(4 + group, group, dot(hidden, w_down_v[...]), down_send, down_recv)
-    for group in range(2):
-        own = block(group, tp)
-        down_sum = sum_total(4 + group, group, down_send, down_recv)
-        mixed[own] = (mid_all[own].astype(f32) + down_sum).astype(bf16)
-        share_start(6 + group, group, mixed)
-    for count, sent in unsent:
-        lax.fori_loop(1, count, sent, 0)
-    for group in range(2):
-        shared(6 + group, group, mixed)
+    hidden = gathered(3, hidden_all)
+    down_part = dot(hidden, w_down_v[...])
+    down_sum = tp_total(5, down_part, part_f32, down_swap, down_swapped, down_quads)
+    mixed[core] = (mid_all[core].astype(f32) + down_sum).astype(bf16)
+    mixed_arrived = tp_share(9, mixed)
+    mixed_arrived()
+    all_sent()
 
 
 def write_out(count, *refs):
-    sources, targets, sem = refs[:count], refs[count : 2 * count], refs[-1]
+    pairs = list(zip(refs[:count], refs[count : 2 * count]))
+    sem = refs[-1]
+    source, target = pairs.pop(1)
+    pairs += [(source.at[one], target.at[one]) for one in range(source.shape[0])]
     copies = [
         pltpu.make_async_copy(source, target, sem.at[place])
-        for place, (source, target) in enumerate(zip(sources, targets))
+        for place, (source, target) in enumerate(pairs)
     ]
     for copy in copies:
         copy.start()
@@ -433,8 +406,8 @@
             args[place] = args[place].T
         tokens, w_query, w_value, state_c, w_gateff = (args[i] for i in (0, 2, 4, 8, 13))
         batch, width = tokens.shape
-        rows = batch // kv_n
-        args[0] = tokens.reshape(kv_n, rows, width)
+        rows, half = batch // kv_n, batch // 2
+        args[0] = tokens.reshape(2, half, width)
         value_size, query_size = state_c.shape[2:]
         ff = w_gateff.shape[0]
         ff_pad = up_to_lanes(ff)
@@ -442,7 +415,7 @@
         heads_all = args[7].shape[1]
         V = pltpu.VMEM
         scratch = [
-            V((kv_n, rows, width), bf16),
+            V((2, half, width), bf16),
             V((1, width), f32),
             V((width, proj_width), bf16),
             V((2 * heads_all, width), bf16),
@@ -452,31 +425,34 @@
             V((1, rows), f32),
             V((value_size, width), bf16),
             V((1, width), f32),
-            V((ff, width), bf16),
-            V((ff, width), bf16),
+            V((ff_pad, width), bf16),
+            V((ff_pad, width), bf16),
             V((ff, width), bf16),
             V((rows, value_size, query_size), bf16),
             V((kv_n, rows, proj_width + LANES), bf16),
             V((kv_n, rows, proj_width + LANES), bf16),
             V((kv_n, rows, value_size), bf16),
-            V((kv_n, rows, width), bf16),
-            V((2, tp_n, rows, width), bf16),
-            V((kv_n, rows, width), bf16),
-            V((kv_n, rows, 2 * ff_pad + LANES), bf16),
-            V((kv_n, rows, 2 * ff_pad + LANES), bf16),
+            V((2, half, width), f32),
+            V((half, width), bf16),
+            V((half, width), bf16),
+            V((tp_n // 2, half, width), bf16),
+            V((2, half, width), bf16),
+            V((kv_n, rows, 2 * ff_pad), bf16),
+            V((kv_n, rows, 2 * ff_pad), bf16),
             V((kv_n, rows, ff), bf16),
-            V((kv_n, rows, width), bf16),
-            V((2, tp_n, rows, width), bf16),
+            V((half, width), bf16),
+            V((half, width), bf16),
+            V((tp_n // 2, half, width), bf16),
             pltpu.SemaphoreType.DMA((16,)),
             pltpu.SemaphoreType.DMA((4, kv_n)),
             pltpu.SemaphoreType.DMA((4, kv_n)),
-            pltpu.SemaphoreType.DMA((8, tp_n)),
-            pltpu.SemaphoreType.DMA((8, tp_n)),
+            pltpu.SemaphoreType.DMA((10,)),
+            pltpu.SemaphoreType.DMA((10,)),
         ]
         anywhere = pl.BlockSpec(memory_space=pl.ANY)
         inside = pl.BlockSpec(memory_space=pltpu.VMEM)
         results = (
-            ((kv_n, rows, width), bf16),
+            ((2, half, width), bf16),
             (state_c.shape, f32),
             (args[9].shape, f32),
             (args[10].shape, f32),
@@ -496,7 +472,7 @@
             out_shape=tuple(jax.ShapeDtypeStruct(shape, dtype) for shape, dtype in results),
             in_specs=[inside] * len(outs),
             out_specs=(anywhere,) * len(outs),
-            scratch_shapes=[pltpu.SemaphoreType.DMA((len(outs),))],
+            scratch_shapes=[pltpu.SemaphoreType.DMA((len(outs) - 1 + rows,))],
             compiler_params=pltpu.CompilerParams(vmem_limit_bytes=1024 * 1024),
         )(*outs)
         return (outs[0].reshape(batch, width), outs[1], outs[2], outs[3].T)

time: 60 us -> 54.7 us (0.912)
  Pallas kernels: 59.3 us -> 53.9 us
    pallas_call x1, Pallas kernels: 57.2 us -> 51.8 us  [per_device(): pl.pallas_call(functools.partial(layer, kv_n, tp_n), out_shape=tuple((V(s...]
where the time goes in v4:
time: 54.7 us; the launch traced here: 54.6 us
  Pallas kernels  53.9 us (99%)
  between operations  0.65 us (1%)
    pallas_call x1, Pallas kernels, per_device(): pl.pallas_call(functools.partial(layer, kv_n, tp_n), out_shape=tuple((V(s...  51.8 us
    pallas_call x1, Pallas kernels, per_device(): pl.pallas_call(functools.partial(write_out, len(outs)), out_shape=tuple((...  2.13 us

profile of v4, /device:TPU:1, one launch (start us, length us, event | category | flops | bytes accessed | tf_op | source)
XLA Modules:
  0.0 54.6 jit_solution(10119600577915920408)
XLA Ops:
  0.6 51.8 %shard_map.183 = (bf16[2,64,256]{2,1,0:T(8,128)(2,1)S(1)}, f32[8,1,512,256]{3,2,1,0:T(8,128)S(1)}, f32[8,1,256]{2,1,0:T(1,128)S(1)}, f32[1,8]{1,0:T(1,128)S(1)}) custom-call(bf16[2,64,256]{2,1,0:T(8,128)(2,1)} %bitcast.13, f32[1,256]{1,0:T(1,128)} %bitcast.14, bf16[256,256]{1,0:T(8,128)(2,1)} %w_query.1, bf16[256,256]{1,0:T(8,128)(2,1)} %w_key.1, ...), custom_call_target="tpu_custom_call" | custom-call | tf_op jit(solution)/shard_map/pallas_call | solution.py:460
  52.5 2.1 %shard_map.184 = (bf16[2,64,256]{2,1,0:T(8,128)(2,1)}, f32[8,1,512,256]{3,2,1,0:T(8,128)}, f32[8,1,256]{2,1,0:T(1,128)}, f32[1,8]{1,0:T(1,128)}) custom-call(bf16[2,64,256]{2,1,0:T(8,128)(2,1)S(1)} %get-tuple-element.12.refs_0_, f32[8,1,512,256]{3,2,1,0:T(8,128)S(1)} %get-tuple-element.13.refs_1_, f32[8,1,256]{2,1,0:T(1,128)S(1)} %get-tuple-element.14.refs_2_, ...), custom_call_target="tpu_custom_call" | custom-call | tf_op jit(solution)/shard_map/pallas_call | solution.py:470

commit v5 on v4

v5 whole, which is shorter than its diff:
```python
import functools

import jax
import jax.numpy as jnp
from jax import lax
from jax.experimental import pallas as pl
from jax.experimental.pallas import tpu as pltpu
from jax.sharding import PartitionSpec as P

MESH = pl.DeviceIdType.MESH
norm_floor = 1e-05
f32 = jnp.float32
bf16 = jnp.bfloat16
LANES = 128


def up_to_lanes(length):
    return (length + LANES - 1) // LANES * LANES


def dot(a, b):
    return jnp.dot(a, b, preferred_element_type=f32)


def dot_rows(a, b):
    return lax.dot_general(a, b, (((1,), (1,)), ((), ())), preferred_element_type=f32)


def lane_ids(rows):
    return lax.broadcasted_iota(jnp.int32, (rows, LANES), 1)


def layer(
    kv_n,
    tp_n,
    chunks,
    tokens,
    attn_gain,
    w_query,
    w_key,
    w_value,
    w_outgate,
    w_gates,
    forget_bias,
    state_c,
    state_n,
    state_m,
    w_output,
    mlp_gain,
    w_gateff,
    w_upff,
    w_downff,
    mixed,
    new_c,
    new_n,
    new_m,
    tok_v,
    gains_v,
    w_proj_v,
    w_gates_v,
    bias_v,
    c_v,
    n_v,
    m_v,
    w_out_v,
    w_ff_v,
    w_down_v,
    c_short,
    qk_send,
    qk_recv,
    vo_send,
    vo_recv,
    head_all,
    part_f32,
    attn_swap,
    attn_swapped,
    attn_quads,
    mid_all,
    ff_send_0,
    ff_recv_0,
    ff_send_1,
    ff_recv_1,
    hidden_0,
    hidden_1,
    down_swap,
    down_swapped,
    down_quads,
    in_sem,
    kv_send_sem,
    kv_recv_sem,
    tp_send_sem,
    tp_recv_sem,
):
    kv = lax.axis_index("kv")
    tp = lax.axis_index("tp")
    _, rows, width = tok_v.shape
    batch = kv_n * rows
    half = batch // 2
    places = kv_n // 2
    width_all = width * kv_n
    heads_all = bias_v.shape[1]
    value_size, query_size = c_v.shape[1:]
    qk_width = 2 * query_size
    vo_width = 2 * value_size

    side = 4
    near = {0: 0, 1: 1, 2: 2, 3: 1}
    kv_z, kv_y = kv // side, lax.rem(kv, side)
    ring, core = tp // 2, lax.rem(tp, 2)
    partner = ring * 2 + (1 - core)

    def far_first(offsets):
        return sorted(offsets, key=lambda offset: -near[offset[0]] - near[offset[1]])

    square = [(a, b) for a in range(side) for b in range(side)]
    around = far_first([offset for offset in square if offset != (0, 0)])
    even = far_first([offset for offset in square if sum(offset) % 2 == 0])
    odd = far_first([offset for offset in square if sum(offset) % 2 == 1])
    colour = lax.rem(kv_z + kv_y, 2)

    def kv_peer(first, second):
        return lax.rem(kv_z + first, side) * side + lax.rem(kv_y + second, side)

    barrier = pltpu.get_barrier_semaphore()

    for offset in around:
        pl.semaphore_signal(
            barrier, inc=1, device_id={"kv": kv_peer(*offset)}, device_id_type=MESH
        )
    tp_peers = [partner] + [lax.rem(ring + offset, side) * 2 + core for offset in (1, 2, 3)]
    for peer in tp_peers:
        pl.semaphore_signal(barrier, inc=1, device_id={"tp": peer}, device_id_type=MESH)

    loads = []

    def load(*pairs, whole=None):
        sem = in_sem.at[len(loads)]
        loads.append(sem)
        for source, target in pairs:
            pltpu.make_async_copy(source, target, sem).start()
        whole = pairs[0][1] if whole is None else whole
        return pltpu.make_async_copy(whole, whole, sem).wait

    wait_tok = load((tokens, tok_v))
    wait_gains = load((attn_gain, gains_v.at[0]), (mlp_gain, gains_v.at[1]), whole=gains_v)
    wait_gates = load((w_gates.at[:, pl.ds(pl.multiple_of(kv * width, width), width)], w_gates_v))
    pairs, at = [], 0
    for weight in (w_query, w_key, w_value, w_outgate):
        columns = weight.shape[1]
        pairs.append((weight, w_proj_v.at[:, pl.ds(at, columns)]))
        at += columns
    wait_proj = load(*pairs, whole=w_proj_v)
    wait_c = load((state_c.at[:, 0], c_v))
    wait_cell = [load((state_n, n_v)), load((state_m, m_v)), load((forget_bias, bias_v))]
    wait_out = load((w_output, w_out_v))
    ff = w_gateff.shape[0]
    ff_rows = w_ff_v.at[:, pl.ds(0, ff)]
    wait_ff = load((w_gateff, ff_rows.at[0]), (w_upff, ff_rows.at[1]), whole=ff_rows)
    wait_down = load((w_downff, w_down_v))

    def kv_copy(phase, source, target, peer):
        return pltpu.make_async_remote_copy(
            src_ref=source,
            dst_ref=target,
            send_sem=kv_send_sem.at[phase],
            recv_sem=kv_recv_sem.at[phase],
            device_id={"kv": peer},
            device_id_type=MESH,
        )

    others = pl.ds(0, kv_n - 1)
    unsent = []

    def all_sent():
        for wait in unsent:
            wait()
        unsent.clear()

    def kv_all(phase, send, recv):
        return kv_copy(phase, send.at[others], recv.at[others], kv_peer(0, 1))

    def scatter_one(phase, peer, send, recv):
        return kv_copy(phase, send.at[peer], recv.at[kv], peer)

    def scatter_all(phase, send, recv):
        for offset in around:
            scatter_one(phase, kv_peer(*offset), send, recv).start()

    def scatter_total(phase, send, recv):
        recv[kv] = send[kv]
        copies = kv_all(phase, send, recv)
        copies.wait_recv()
        unsent.append(copies.wait_send)
        total = recv[0].astype(f32)
        for peer in range(1, kv_n):
            total = total + recv[peer].astype(f32)
        return total

    def gather_start(phase, blocks):
        for offset in around:
            kv_copy(phase, blocks.at[kv], blocks.at[kv], kv_peer(*offset)).start()

    def block(group, place):
        first = place // 2
        return first * side + 2 * (place % 2) + (first + group) % 2

    def gathered(phase, blocks):
        copies = kv_all(phase, blocks, blocks)
        copies.wait_recv()
        unsent.append(copies.wait_send)
        parts = [blocks[block(group, place)] for group in range(2) for place in range(places)]
        return jnp.concatenate([part.astype(f32) for part in parts], axis=0).astype(bf16)

    def tp_copy(place, source, target, peer):
        return pltpu.make_async_remote_copy(
            src_ref=source,
            dst_ref=target,
            send_sem=tp_send_sem.at[place],
            recv_sem=tp_recv_sem.at[place],
            device_id={"tp": peer},
            device_id_type=MESH,
        )

    def tp_total(first, part, swap_send, swap_recv, quads):
        part_f32[...] = part.reshape(2, half, width)
        swap_send[...] = part_f32[1 - core].astype(bf16)
        swap = tp_copy(first, swap_send, swap_recv, partner)
        swap.start()
        swap.wait_recv()
        quads[ring] = (part_f32[core] + swap_recv[...].astype(f32)).astype(bf16)
        for offset in (2, 1, 3):
            peer = lax.rem(ring + offset, side) * 2 + core
            tp_copy(first + 1, quads.at[ring], quads.at[ring], peer).start()
        all_sent()
        three = quads.at[pl.ds(0, side - 1)]
        copies = tp_copy(first + 1, three, three, partner)
        copies.wait_recv()
        unsent.extend((swap.wait_send, copies.wait_send))
        total = quads[0].astype(f32)
        for place in range(1, side):
            total = total + quads[place].astype(f32)
        return total

    def tp_share(place, halves):
        copy = tp_copy(place, halves.at[core], halves.at[core], partner)
        copy.start()
        unsent.append(copy.wait_send)
        other = halves.at[1 - core]
        return tp_copy(place, other, other, partner).wait_recv

    wait_tok()
    wait_gains()
    tok_float = tok_v[...].astype(f32).reshape(batch, width)
    squares_one = jnp.sum(tok_float * tok_float, axis=1, keepdims=True)
    normed_one = (tok_float * gains_v[0]).astype(bf16)
    lanes = lane_ids(batch)
    gate_row = lax.broadcasted_iota(jnp.int32, (LANES, 2 * heads_all), 1)
    gate_lane = lax.broadcasted_iota(jnp.int32, (LANES, 2 * heads_all), 0)
    wanted = jnp.where(
        (gate_lane == 0) | (gate_lane == 3),
        tp,
        jnp.where((gate_lane == 1) | (gate_lane == 4), heads_all + tp, -1),
    )
    pick = jnp.where(gate_row == wanted, 1.0, 0.0).astype(bf16)
    wait_gates()
    gate_weight = dot(pick, w_gates_v[...]).astype(bf16)
    extra = dot_rows(normed_one, gate_weight)
    extra = jnp.where((lanes == 2) | (lanes == 5), squares_one, extra)
    extra_short = extra.astype(bf16).astype(f32)
    extra = jnp.where(lanes < 3, extra_short, extra - extra_short)
    qk_send[:, :, pl.ds(qk_width, LANES)] = extra.reshape(kv_n, rows, LANES).astype(bf16)
    wait_proj()
    step = 512
    for target, base, length in ((qk_send, 0, qk_width), (vo_send, qk_width, vo_width)):
        for at in range(0, length, step):
            part = dot(normed_one, w_proj_v[:, pl.ds(base + at, step)])
            target[:, :, pl.ds(at, step)] = part.reshape(kv_n, rows, step).astype(bf16)

    pl.semaphore_wait(barrier, kv_n + len(tp_peers) - 1)
    scatter_all(0, qk_send, qk_recv)
    scatter_all(1, vo_send, vo_recv)

    wait_c()
    for one in range(rows):
        c_short[one] = c_v[one].astype(bf16)
    for wait in wait_cell:
        wait()

    qk_rows = scatter_total(0, qk_send, qk_recv)
    extra = qk_rows[:, qk_width:]
    lanes = lane_ids(rows)

    def picked(lane):
        chosen = (lanes == lane) | (lanes == lane + 3)
        return jnp.sum(jnp.where(chosen, extra, 0.0), axis=1, keepdims=True)

    scale_one = lax.rsqrt(picked(2) / width_all + norm_floor)
    query = qk_rows[:, :query_size] * (scale_one * query_size ** (-0.5))
    key_vec = qk_rows[:, query_size:qk_width] * scale_one
    head_lane = lax.broadcasted_iota(jnp.int32, (1, heads_all), 1)
    bias = jnp.sum(jnp.where(head_lane == tp, bias_v[...], 0.0), axis=1, keepdims=True)
    log_input = picked(0) * scale_one
    forget_pre = picked(1) * scale_one + bias
    log_forget = -(jnp.maximum(-forget_pre, 0.0) + jnp.log1p(jnp.exp(-jnp.abs(forget_pre))))
    row_at = lax.broadcasted_iota(jnp.int32, (rows, rows), 0)
    same = row_at == lax.broadcasted_iota(jnp.int32, (rows, rows), 1)
    m_column = jnp.sum(jnp.where(same, m_v[...], 0.0), axis=1, keepdims=True)
    carried = log_forget + m_column
    m_next = jnp.maximum(carried, log_input)
    keep = jnp.exp(carried - m_next)
    admit = jnp.exp(log_input - m_next)
    n_next = keep * n_v[:, 0, :] + admit * key_vec
    denom = jnp.maximum(
        jnp.abs(jnp.sum(n_next * query, axis=1, keepdims=True)), jnp.exp(-m_next)
    )
    key_query = jnp.sum(key_vec * query, axis=1, keepdims=True)
    query_short = query.astype(bf16)
    query_rest = (query - query_short.astype(f32)).astype(bf16)
    row_ids = lax.broadcasted_iota(jnp.int32, (rows, value_size), 0)
    read = jnp.zeros((rows, value_size), f32)
    query_both = jnp.concatenate([query_short.astype(f32), query_rest.astype(f32)], axis=0).astype(bf16)
    for one in range(rows):
        product = dot_rows(query_both, c_short[one])
        read = jnp.where(row_ids == one, product[:rows] + product[rows:], read)
    kept_read = keep * read
    vo_rows = scatter_total(1, vo_send, vo_recv)
    admitted = (admit * scale_one) * vo_rows[:, :value_size]
    out_pre = vo_rows[:, value_size:] * scale_one
    numer = kept_read + admitted * key_query
    head_all[kv] = (jax.nn.sigmoid(out_pre) * numer / denom).astype(bf16)
    gather_start(2, head_all)

    new_n[:, 0, :] = n_next
    new_m[...] = jnp.sum(jnp.where(same, m_next, 0.0), axis=0, keepdims=True)
    admitted_column = admitted.T
    for one in range(rows):
        new_c[one, 0] = (
            keep[one : one + 1, :] * c_v[one]
            + admitted_column[:, one : one + 1] * key_vec[one : one + 1, :]
        )

    wait_out()
    heads = gathered(2, head_all)
    attn_part = dot(heads, w_out_v[...])
    attn_mix = tp_total(0, attn_part, attn_swap, attn_swapped, attn_quads)
    tok_half = [tok_v[block(core, place)].astype(f32) for place in range(places)]
    mid_all[core] = (jnp.concatenate(tok_half, axis=0) + attn_mix).astype(bf16)
    mid_arrived = tp_share(2, mid_all)
    wait_ff()

    lanes = lane_ids(half)
    (start_0, ff_0, wide_0), (start_1, ff_1, wide_1) = chunks

    def normed(at_half):
        mid_float = mid_all[at_half].astype(f32)
        squares = jnp.sum(mid_float * mid_float, axis=1, keepdims=True)
        return squares, (mid_float * gains_v[1]).astype(bf16)

    def ff_products(source, start, wide, send, at_half, extra):
        count = source.shape[0] // rows
        for which in range(2):
            for at in range(0, wide, step):
                columns = min(step, wide - at)
                weight = w_ff_v[which, pl.ds(start + at, columns), :]
                part = dot_rows(source, weight)
                if extra is not None and which == 0 and at + columns == wide:
                    last = jnp.where(lanes < LANES - 2, part[:, columns - LANES :], extra)
                    if columns > LANES:
                        last = jnp.concatenate([part[:, : columns - LANES], last], axis=1)
                    part = last
                part = part.reshape(count, rows, columns).astype(bf16)
                for place in range(count):
                    group = at_half if count == places else place // places
                    send[block(group, place % places), :, pl.ds(which * wide + at, columns)] = part[place]

    for turn in range(2):
        at_half = core if turn == 0 else 1 - core
        if turn == 1:
            mid_arrived()
        squares_two, normed_two = normed(at_half)
        squares_short = squares_two.astype(bf16).astype(f32)
        extra = jnp.where(lanes == LANES - 2, squares_short, squares_two - squares_short)
        ff_products(normed_two, start_0, wide_0, ff_send_0, at_half, extra)
        mine = colour == at_half
        for at_even, at_odd in zip(even, odd):
            peer = kv_peer(
                jnp.where(mine, at_even[0], at_odd[0]), jnp.where(mine, at_even[1], at_odd[1])
            )
            copy = scatter_one(3, peer, ff_send_0, ff_recv_0)
            if at_even == (0, 0):
                pl.when(jnp.logical_not(mine))(copy.start)
            else:
                copy.start()
    normed_two = jnp.concatenate([normed(0)[1], normed(1)[1]], axis=0)
    ff_products(normed_two, start_1, wide_1, ff_send_1, None, None)
    scatter_all(4, ff_send_1, ff_recv_1)

    def activated(total, columns, wide, scale):
        gate = total[:, :columns] * scale
        up = total[:, wide : wide + columns] * scale
        return (gate / (1.0 + jnp.exp(-gate)) * up).astype(bf16)

    total_0 = scatter_total(3, ff_send_0, ff_recv_0)
    rows_two = jnp.sum(total_0[:, wide_0 - 2 : wide_0], axis=1, keepdims=True)
    scale_two = lax.rsqrt(rows_two / width_all + norm_floor)
    hidden_0[kv] = activated(total_0, ff_0, wide_0, scale_two)
    gather_start(5, hidden_0)
    total_1 = scatter_total(4, ff_send_1, ff_recv_1)
    hidden_1[kv] = activated(total_1, ff_1, wide_1, scale_two)
    gather_start(6, hidden_1)

    wait_down()
    down_part = dot(gathered(5, hidden_0), w_down_v[pl.ds(start_0, ff_0), :])
    down_part = down_part + dot(gathered(6, hidden_1), w_down_v[pl.ds(start_1, ff_1), :])
    down_sum = tp_total(3, down_part, down_swap, down_swapped, down_quads)
    mixed[core] = (mid_all[core].astype(f32) + down_sum).astype(bf16)
    mixed_arrived = tp_share(5, mixed)
    mixed_arrived()
    all_sent()


def write_out(mixed, new_c, new_n, new_m, mixed_to, c_to, n_to, m_to, sem):
    kv_n = mixed_to.shape[0]
    rows, side = mixed_to.shape[1], 4
    groups = ([(new_c.at[one], c_to.at[one]) for one in range(new_c.shape[0])], [], [], [])
    groups[1].append((new_n, n_to))
    groups[2].append((new_m, m_to))
    for block in range(kv_n):
        first, second = block // side, block % side
        place = (first * 2 + second // 2) * rows
        source = mixed.at[(first + second) % 2, pl.ds(place, rows)]
        groups[3].append((source, mixed_to.at[block]))
    for at, pairs in enumerate(groups):
        for source, target in pairs:
            pltpu.make_async_copy(source, target, sem.at[at]).start()
    for at, whole in enumerate((new_c, new_n, new_m, mixed)):
        pltpu.make_async_copy(whole, whole, sem.at[at]).wait()


def solution(mesh):
    kv_n, tp_n = mesh.shape["kv"], mesh.shape["tp"]

    def per_device(*args):
        args = list(args)
        for place in (1, 7, 12):
            args[place] = args[place].reshape(1, -1)
        for place in (6, 10, 13, 14):
            args[place] = args[place].T
        tokens, w_query, w_value, state_c, w_gateff = (args[i] for i in (0, 2, 4, 8, 13))
        batch, width = tokens.shape
        rows, half = batch // kv_n, batch // 2
        args[0] = tokens.reshape(kv_n, rows, width)
        value_size, query_size = state_c.shape[2:]
        ff = w_gateff.shape[0]
        ff_pad = up_to_lanes(ff)
        second = 512
        chunks = ((second, ff - second, ff_pad - second), (0, second, second))
        proj_width = 2 * query_size + 2 * value_size
        heads_all = args[7].shape[1]
        V = pltpu.VMEM
        scratch = [
            V((kv_n, rows, width), bf16),
            V((2, 1, width), f32),
            V((width, proj_width), bf16),
            V((2 * heads_all, width), bf16),
            V((1, heads_all), f32),
            V((rows, value_size, query_size), f32),
            V((rows, 1, query_size), f32),
            V((1, rows), f32),
            V((value_size, width), bf16),
            V((2, ff_pad, width), bf16),
            V((ff, width), bf16),
            V((rows, value_size, query_size), bf16),
            V((kv_n, rows, 2 * query_size + LANES), bf16),
            V((kv_n, rows, 2 * query_size + LANES), bf16),
            V((kv_n, rows, 2 * value_size), bf16),
            V((kv_n, rows, 2 * value_size), bf16),
            V((kv_n, rows, value_size), bf16),
            V((2, half, width), f32),
            V((half, width), bf16),
            V((half, width), bf16),
            V((tp_n // 2, half, width), bf16),
            V((2, half, width), bf16),
            V((kv_n, rows, 2 * chunks[0][2]), bf16),
            V((kv_n, rows, 2 * chunks[0][2]), bf16),
            V((kv_n, rows, 2 * chunks[1][2]), bf16),
            V((kv_n, rows, 2 * chunks[1][2]), bf16),
            V((kv_n, rows, chunks[0][1]), bf16),
            V((kv_n, rows, chunks[1][1]), bf16),
            V((half, width), bf16),
            V((half, width), bf16),
            V((tp_n // 2, half, width), bf16),
            pltpu.SemaphoreType.DMA((11,)),
            pltpu.SemaphoreType.DMA((7,)),
            pltpu.SemaphoreType.DMA((7,)),
            pltpu.SemaphoreType.DMA((6,)),
            pltpu.SemaphoreType.DMA((6,)),
        ]
        anywhere = pl.BlockSpec(memory_space=pl.ANY)
        inside = pl.BlockSpec(memory_space=pltpu.VMEM)
        results = (
            ((2, half, width), bf16),
            (state_c.shape, f32),
            (args[9].shape, f32),
            (args[10].shape, f32),
        )
        outs = pl.pallas_call(
            functools.partial(layer, kv_n, tp_n, chunks),
            out_shape=tuple(V(shape, dtype) for shape, dtype in results),
            in_specs=[anywhere] * len(args),
            out_specs=(inside,) * 4,
            scratch_shapes=scratch,
            compiler_params=pltpu.CompilerParams(
                collective_id=0, has_side_effects=True, vmem_limit_bytes=58 * 1024 * 1024
            ),
        )(*args)
        results = (((kv_n, rows, width), bf16), *results[1:])
        outs = pl.pallas_call(
            write_out,
            out_shape=tuple(jax.ShapeDtypeStruct(shape, dtype) for shape, dtype in results),
            in_specs=[inside] * len(outs),
            out_specs=(anywhere,) * len(outs),
            scratch_shapes=[pltpu.SemaphoreType.DMA((len(outs),))],
            compiler_params=pltpu.CompilerParams(vmem_limit_bytes=1024 * 1024),
        )(*outs)
        return (outs[0].reshape(batch, width), outs[1], outs[2], outs[3].T)

    placed = (
        P(None, "kv"),
        P("kv"),
        P("kv", "tp"),
        P("kv", "tp"),
        P("kv", "tp"),
        P("kv", "tp"),
        P(),
        P(),
        P("kv", "tp", None, None),
        P("kv", "tp", None),
        P("kv", "tp"),
        P("tp", "kv"),
        P("kv"),
        P("kv", "tp"),
        P("kv", "tp"),
        P("tp", "kv"),
    )
    return jax.shard_map(
        per_device,
        mesh=mesh,
        in_specs=placed,
        out_specs=(P(None, "kv"), P("kv", "tp", None, None), P("kv", "tp", None), P("kv", "tp")),
        check_vma=False,
    )
```

time: 54.7 us -> 50.1 us (0.916)
  Pallas kernels: 53.9 us -> 49.4 us
    pallas_call x2, Pallas kernels: 53.9 us -> 49.4 us  [the longest x1 47.3 us: per_device(): pl.pallas_call(functools.partial(layer, kv_n, tp_n, chunks), out_shape=tu...]
where the time goes in v5:
time: 50.1 us; the launch traced here: 50 us
  Pallas kernels  49.4 us (99%)
  between operations  0.65 us (1%)
    pallas_call x1, Pallas kernels, per_device(): pl.pallas_call(functools.partial(layer, kv_n, tp_n, chunks), out_shape=tu...  47.3 us
    pallas_call x1, Pallas kernels, per_device(): pl.pallas_call(write_out, out_shape=tuple((jax.ShapeDtypeStruct(shape, dt...  2.07 us

profile of v5, /device:TPU:1, one launch (start us, length us, event | category | flops | bytes accessed | tf_op | source)
XLA Modules:
  0.0 50.0 jit_solution(16457297886667919350)
XLA Ops:
  0.6 47.3 %shard_map.183 = (bf16[2,64,256]{2,1,0:T(8,128)(2,1)S(1)}, f32[8,1,512,256]{3,2,1,0:T(8,128)S(1)}, f32[8,1,256]{2,1,0:T(1,128)S(1)}, f32[1,8]{1,0:T(1,128)S(1)}) custom-call(bf16[16,8,256]{2,1,0:T(8,128)(2,1)} %bitcast.13, f32[1,256]{1,0:T(1,128)} %bitcast.14, bf16[256,256]{1,0:T(8,128)(2,1)} %w_query.1, bf16[256,256]{1,0:T(8,128)(2,1)} %w_key.1, ...), custom_call_target="tpu_custom_call" | custom-call | tf_op jit(solution)/shard_map/pallas_call | solution.py:507
  48.0 2.1 %shard_map.184 = (bf16[16,8,256]{2,1,0:T(8,128)(2,1)}, f32[8,1,512,256]{3,2,1,0:T(8,128)}, f32[8,1,256]{2,1,0:T(1,128)}, f32[1,8]{1,0:T(1,128)}) custom-call(bf16[2,64,256]{2,1,0:T(8,128)(2,1)S(1)} %get-tuple-element.12.mixed, f32[8,1,512,256]{3,2,1,0:T(8,128)S(1)} %get-tuple-element.13.new_c, f32[8,1,256]{2,1,0:T(1,128)S(1)} %get-tuple-element.14.new_n, ...), custom_call_target="tpu_custom_call" | custom-call | tf_op jit(solution)/shard_map/pallas_call | solution.py:518

commit v6 on v5

--- a/solution.py
+++ b/solution.py
@@ -113,6 +113,9 @@
         return sorted(offsets, key=lambda offset: -near[offset[0]] - near[offset[1]])
 
     square = [(a, b) for a in range(side) for b in range(side)]
+    spread = [(2, 2), (1, 2), (3, 2), (2, 1), (2, 3), (1, 1), (3, 3), (1, 3), (3, 1), (0, 2), (2, 0)]
+    spread += [(0, 1), (0, 3), (1, 0), (3, 0)]
+    first_up = sorted(range(kv_n), key=lambda at: at // side + at % side)
     around = far_first([offset for offset in square if offset != (0, 0)])
     even = far_first([offset for offset in square if sum(offset) % 2 == 0])
     odd = far_first([offset for offset in square if sum(offset) % 2 == 1])
@@ -182,9 +185,16 @@
     def scatter_one(phase, peer, send, recv):
         return kv_copy(phase, send.at[peer], recv.at[kv], peer)
 
-    def scatter_all(phase, send, recv):
-        for offset in around:
-            scatter_one(phase, kv_peer(*offset), send, recv).start()
+    def in_order(copy_to, order):
+        if order is None or isinstance(order[0], tuple):
+            for offset in order or around:
+                copy_to(kv_peer(*offset)).start()
+        else:
+            for peer in order:
+                pl.when(kv != peer)(copy_to(peer).start)
+
+    def scatter_all(phase, send, recv, order=None):
+        in_order(lambda peer: scatter_one(phase, peer, send, recv), order)
 
     def scatter_total(phase, send, recv):
         recv[kv] = send[kv]
@@ -196,9 +206,8 @@
             total = total + recv[peer].astype(f32)
         return total
 
-    def gather_start(phase, blocks):
-        for offset in around:
-            kv_copy(phase, blocks.at[kv], blocks.at[kv], kv_peer(*offset)).start()
+    def gather_start(phase, blocks, order=None):
+        in_order(lambda peer: kv_copy(phase, blocks.at[kv], blocks.at[kv], peer), order)
 
     def block(group, place):
         first = place // 2
@@ -393,7 +402,7 @@
                 copy.start()
     normed_two = jnp.concatenate([normed(0)[1], normed(1)[1]], axis=0)
     ff_products(normed_two, start_1, wide_1, ff_send_1, None, None)
-    scatter_all(4, ff_send_1, ff_recv_1)
+    scatter_all(4, ff_send_1, ff_recv_1, spread)
 
     def activated(total, columns, wide, scale):
         gate = total[:, :columns] * scale
@@ -404,10 +413,10 @@
     rows_two = jnp.sum(total_0[:, wide_0 - 2 : wide_0], axis=1, keepdims=True)
     scale_two = lax.rsqrt(rows_two / width_all + norm_floor)
     hidden_0[kv] = activated(total_0, ff_0, wide_0, scale_two)
-    gather_start(5, hidden_0)
+    gather_start(5, hidden_0, first_up)
     total_1 = scatter_total(4, ff_send_1, ff_recv_1)
     hidden_1[kv] = activated(total_1, ff_1, wide_1, scale_two)
-    gather_start(6, hidden_1)
+    gather_start(6, hidden_1, first_up)
 
     wait_down()
     down_part = dot(gathered(5, hidden_0), w_down_v[pl.ds(start_0, ff_0), :])
@@ -422,7 +431,7 @@
 def write_out(mixed, new_c, new_n, new_m, mixed_to, c_to, n_to, m_to, sem):
     kv_n = mixed_to.shape[0]
     rows, side = mixed_to.shape[1], 4
-    groups = ([(new_c.at[one], c_to.at[one]) for one in range(new_c.shape[0])], [], [], [])
+    groups = ([(new_c, c_to)], [], [], [])
     groups[1].append((new_n, n_to))
     groups[2].append((new_m, m_to))
     for block in range(kv_n):
@@ -453,7 +462,7 @@
         value_size, query_size = state_c.shape[2:]
         ff = w_gateff.shape[0]
         ff_pad = up_to_lanes(ff)
-        second = 512
+        second = 640
         chunks = ((second, ff - second, ff_pad - second), (0, second, second))
         proj_width = 2 * query_size + 2 * value_size
         heads_all = args[7].shape[1]

time: 50.1 us -> 49.5 us (0.988)
  Pallas kernels: 49.4 us -> 48.7 us
    pallas_call x1, Pallas kernels: 47.3 us -> 46.6 us  [per_device(): pl.pallas_call(functools.partial(layer, kv_n, tp_n, chunks), out_shape=tu...]
where the time goes in v6:
time: 49.5 us; the launch traced here: 49.4 us
  Pallas kernels  48.7 us (98%)
  between operations  0.65 us (1%)
    pallas_call x1, Pallas kernels, per_device(): pl.pallas_call(functools.partial(layer, kv_n, tp_n, chunks), out_shape=tu...  46.6 us
    pallas_call x1, Pallas kernels, per_device(): pl.pallas_call(write_out, out_shape=tuple((jax.ShapeDtypeStruct(shape, dt...  2.07 us

profile of v6, /device:TPU:1, one launch (start us, length us, event | category | flops | bytes accessed | tf_op | source)
XLA Modules:
  0.0 49.4 jit_solution(15617959168820290749)
XLA Ops:
  0.6 46.6 %shard_map.183 = (bf16[2,64,256]{2,1,0:T(8,128)(2,1)S(1)}, f32[8,1,512,256]{3,2,1,0:T(8,128)S(1)}, f32[8,1,256]{2,1,0:T(1,128)S(1)}, f32[1,8]{1,0:T(1,128)S(1)}) custom-call(bf16[16,8,256]{2,1,0:T(8,128)(2,1)} %bitcast.13, f32[1,256]{1,0:T(1,128)} %bitcast.14, bf16[256,256]{1,0:T(8,128)(2,1)} %w_query.1, bf16[256,256]{1,0:T(8,128)(2,1)} %w_key.1, ...), custom_call_target="tpu_custom_call" | custom-call | tf_op jit(solution)/shard_map/pallas_call | solution.py:516
  47.3 2.1 %shard_map.184 = (bf16[16,8,256]{2,1,0:T(8,128)(2,1)}, f32[8,1,512,256]{3,2,1,0:T(8,128)}, f32[8,1,256]{2,1,0:T(1,128)}, f32[1,8]{1,0:T(1,128)}) custom-call(bf16[2,64,256]{2,1,0:T(8,128)(2,1)S(1)} %get-tuple-element.12.mixed, f32[8,1,512,256]{3,2,1,0:T(8,128)S(1)} %get-tuple-element.13.new_c, f32[8,1,256]{2,1,0:T(1,128)S(1)} %get-tuple-element.14.new_n, ...), custom_call_target="tpu_custom_call" | custom-call | tf_op jit(solution)/shard_map/pallas_call | solution.py:527

commit v7 on v6

--- a/solution.py
+++ b/solution.py
@@ -116,6 +116,7 @@
     spread = [(2, 2), (1, 2), (3, 2), (2, 1), (2, 3), (1, 1), (3, 3), (1, 3), (3, 1), (0, 2), (2, 0)]
     spread += [(0, 1), (0, 3), (1, 0), (3, 0)]
     first_up = sorted(range(kv_n), key=lambda at: at // side + at % side)
+    first_served = [0, 1, 4, 5, 3, 12, 15, 2, 8, 10, 6, 9, 7, 13, 11, 14]
     around = far_first([offset for offset in square if offset != (0, 0)])
     even = far_first([offset for offset in square if sum(offset) % 2 == 0])
     odd = far_first([offset for offset in square if sum(offset) % 2 == 1])
@@ -337,7 +338,7 @@
     out_pre = vo_rows[:, value_size:] * scale_one
     numer = kept_read + admitted * key_query
     head_all[kv] = (jax.nn.sigmoid(out_pre) * numer / denom).astype(bf16)
-    gather_start(2, head_all)
+    gather_start(2, head_all, spread)
 
     new_n[:, 0, :] = n_next
     new_m[...] = jnp.sum(jnp.where(same, m_next, 0.0), axis=0, keepdims=True)
@@ -416,7 +417,7 @@
     gather_start(5, hidden_0, first_up)
     total_1 = scatter_total(4, ff_send_1, ff_recv_1)
     hidden_1[kv] = activated(total_1, ff_1, wide_1, scale_two)
-    gather_start(6, hidden_1, first_up)
+    gather_start(6, hidden_1, first_served)
 
     wait_down()
     down_part = dot(gathered(5, hidden_0), w_down_v[pl.ds(start_0, ff_0), :])

time: 49.5 us -> 49.4 us (level)
  no operation moved by 1% of the time
where the time goes in v7:
time: 49.4 us; the launch traced here: 49.3 us
  Pallas kernels  48.6 us (98%)
  between operations  0.65 us (1%)
    pallas_call x1, Pallas kernels, per_device(): pl.pallas_call(functools.partial(layer, kv_n, tp_n, chunks), out_shape=tu...  46.5 us
    pallas_call x1, Pallas kernels, per_device(): pl.pallas_call(write_out, out_shape=tuple((jax.ShapeDtypeStruct(shape, dt...  2.07 us

profile of v7, /device:TPU:1, one launch (start us, length us, event | category | flops | bytes accessed | tf_op | source)
XLA Modules:
  0.0 49.3 jit_solution(5500983773934265375)
XLA Ops:
  0.6 46.5 %shard_map.183 = (bf16[2,64,256]{2,1,0:T(8,128)(2,1)S(1)}, f32[8,1,512,256]{3,2,1,0:T(8,128)S(1)}, f32[8,1,256]{2,1,0:T(1,128)S(1)}, f32[1,8]{1,0:T(1,128)S(1)}) custom-call(bf16[16,8,256]{2,1,0:T(8,128)(2,1)} %bitcast.13, f32[1,256]{1,0:T(1,128)} %bitcast.14, bf16[256,256]{1,0:T(8,128)(2,1)} %w_query.1, bf16[256,256]{1,0:T(8,128)(2,1)} %w_key.1, ...), custom_call_target="tpu_custom_call" | custom-call | tf_op jit(solution)/shard_map/pallas_call | solution.py:517
  47.2 2.1 %shard_map.184 = (bf16[16,8,256]{2,1,0:T(8,128)(2,1)}, f32[8,1,512,256]{3,2,1,0:T(8,128)}, f32[8,1,256]{2,1,0:T(1,128)}, f32[1,8]{1,0:T(1,128)}) custom-call(bf16[2,64,256]{2,1,0:T(8,128)(2,1)S(1)} %get-tuple-element.12.mixed, f32[8,1,512,256]{3,2,1,0:T(8,128)S(1)} %get-tuple-element.13.new_c, f32[8,1,256]{2,1,0:T(1,128)S(1)} %get-tuple-element.14.new_n, ...), custom_call_target="tpu_custom_call" | custom-call | tf_op jit(solution)/shard_map/pallas_call | solution.py:528
